TPU v7x, 512 devices: a whole 4x4x16 slice. The times are simulated.
512 devices in a mesh: kv: 16 (over y, x), tp: 32 (over z, core).
Axes of the slice: x: 4, y: 4, z: 16, core: 2. Of those that a mesh axis runs over, the one named last changes fastest.
Arguments:
- residual: bfloat16 [512, 4096], P(None, ('kv', 'tp')), may hold values from -20 to 20
- mixer_gain: float32 [4096], P('kv'), may hold values from 0.1 to 1.9
- w_query: bfloat16 [4096, 4096], P('kv', 'tp'), may hold values from -0.09375 to 0.09375
- w_forget: bfloat16 [4096, 4096], P('kv', 'tp'), may hold values from -0.09375 to 0.09375
- w_input: bfloat16 [4096, 4096], P('kv', 'tp'), may hold values from -0.09375 to 0.09375
- w_outgate: bfloat16 [4096, 4096], P('kv', 'tp'), may hold values from -0.09375 to 0.09375
- lower_bound: float32 [4096], P('tp'), may hold values from 0.3 to 0.97
- state: float32 [512, 32, 128, 128], P('kv', 'tp'), may hold values from -6 to 6
- head_gain: float32 [128], replicated, may hold values from 0.1 to 1.9
- w_mix_out: bfloat16 [4096, 4096], P('tp', 'kv'), may hold values from -0.09375 to 0.09375
- ffn_gain: float32 [4096], P('kv'), may hold values from 0.1 to 1.9
- w_gate: bfloat16 [4096, 10752], P('kv', 'tp'), may hold values from -0.09375 to 0.09375
- w_up: bfloat16 [4096, 10752], P('kv', 'tp'), may hold values from -0.09375 to 0.09375
- w_down: bfloat16 [10752, 4096], P('tp', 'kv'), may hold values from -0.0625 to 0.0625
Outputs:
- layer_out: bfloat16 [512, 4096], P(None, ('kv', 'tp'))
- new_state: float32 [512, 32, 128, 128], P('kv', 'tp')
All inputs are finite; a program needn't handle non-finite values.
Results may differ from a plain program's by a relative error of at most 0.015.
Values may be sent and summed in bfloat16 or wider, within the bound.
A program may use at most 64 MiB of HBM per device.

v0:
```python
import math

import jax
import jax.numpy as jnp
from jax import lax
from jax.sharding import PartitionSpec as P

D = 4096
DK = 128
DV = 128


EPS = 1e-06


def filled_up(lines, size):
    spare = -lines.shape[0] % size
    if not spare:
        return lines
    return jnp.concatenate([lines, jnp.zeros((spare, *lines.shape[1:]), lines.dtype)])


def in_order(tiles, dim):
    tiles = jnp.moveaxis(tiles, 0, dim)
    shape = tiles.shape
    return tiles.reshape(*shape[:dim], shape[dim] * shape[dim + 1], *shape[dim + 2 :])


def copy_for_each(shard, axis):
    copies = jnp.broadcast_to(shard, (lax.axis_size(axis), *shard.shape))
    return lax.all_to_all(copies, axis, split_axis=0, concat_axis=0, tiled=True)


def collect(shard, axis, dim):
    return in_order(copy_for_each(shard, axis), dim)


def cut_along(shard, dim, size):
    shape = shard.shape
    tiles = shard.reshape(*shape[:dim], size, shape[dim] // size, *shape[dim + 1 :])
    return jnp.moveaxis(tiles, dim, 0)


def summed_on_arrival(shard, axis, dim):
    tiles = cut_along(shard, dim, lax.axis_size(axis))
    arrived = lax.all_to_all(tiles, axis, split_axis=0, concat_axis=0, tiled=True)
    return arrived.astype(jnp.float32).sum(axis=0)


def total_of(shard, axes):
    lines = shard.reshape(-1)
    padded = filled_up(lines, lax.axis_size(axes))
    whole = collect(summed_on_arrival(padded, axes, 0).astype(jnp.bfloat16), axes, 0)
    return lax.slice_in_dim(whole, 0, len(lines)).reshape(shard.shape).astype(jnp.float32)


def sent_together(arrays, axis, dim, along):
    widths = [math.prod(a.shape[along:]) for a in arrays]
    both = jnp.concatenate(
        [a.reshape(*a.shape[:along], w) for a, w in zip(arrays, widths)], axis=along
    )
    result = summed_on_arrival(both, axis, dim)
    tiles = jnp.split(result, [sum(widths[:k]) for k in range(1, len(widths))], axis=along)
    return tuple(
        (b.reshape(*result.shape[:along], *a.shape[along:]) for a, b in zip(arrays, tiles))
    )


def summed_on_arrival_2(shard, axis, dim):
    size = lax.axis_size(axis)
    tiles = lax.all_to_all(cut_along(shard, dim, size), axis, 0, 0, tiled=True)
    return jnp.sum(tiles, axis=0)


def nested_sum(shard, axes):
    lines = shard.reshape(-1, shard.shape[-1])
    padded = filled_up(lines, lax.axis_size(axes))
    whole = collect(summed_on_arrival_2(padded, axes, 0), axes, 0)
    return lax.slice_in_dim(whole, 0, len(lines)).reshape(shard.shape)


def project_row(weight, piece):
    return jnp.dot(piece, weight, preferred_element_type=jnp.float32)


def channel_mix(rows_in, ffn_gain, w_gate, w_up, w_down):
    rows_float = rows_in.astype(jnp.float32)
    squares = jnp.sum(rows_float * rows_float, axis=1)
    scaled = (rows_float * ffn_gain).astype(jnp.bfloat16)
    gate = jnp.dot(scaled, w_gate, preferred_element_type=jnp.float32)
    upper = jnp.dot(scaled, w_up, preferred_element_type=jnp.float32)
    gate, upper, total = (
        total_of(gate.astype(jnp.bfloat16), "kv"),
        total_of(upper.astype(jnp.bfloat16), "kv"),
        total_of(squares.astype(jnp.bfloat16), "kv"),
    )
    inverse = lax.rsqrt(total / D + EPS)[:, None]
    hidden = (jax.nn.silu(gate * inverse) * (upper * inverse)).astype(jnp.bfloat16)
    terms = jnp.dot(hidden, w_down, preferred_element_type=jnp.float32)
    summed = summed_on_arrival(terms.astype(jnp.bfloat16), "tp", 1)
    width = summed.shape[1]
    own = lax.dynamic_slice_in_dim(rows_float, lax.axis_index("tp") * width, width, 1)
    return (own + summed).astype(jnp.bfloat16)


def body(
    residual,
    mixer_gain,
    w_query,
    w_forget,
    w_input,
    w_outgate,
    lower_bound,
    state,
    head_gain,
    w_mix_out,
    ffn_gain,
    w_gate,
    w_up,
    w_down,
):
    local_seqs, local_heads = (state.shape[0], state.shape[1])
    rows = collect(residual, "tp", 1)
    rows_float = rows.astype(jnp.float32)
    squares = jnp.sum(rows_float * rows_float, axis=1)
    scaled = (rows_float * mixer_gain).astype(jnp.bfloat16)
    part_query = jnp.dot(scaled, w_query, preferred_element_type=jnp.float32)
    part_forget = jnp.dot(scaled, w_forget, preferred_element_type=jnp.float32)
    part_value = jnp.dot(scaled, w_input, preferred_element_type=jnp.float32)
    part_gate = jnp.dot(scaled, w_outgate, preferred_element_type=jnp.float32)
    part_query, part_forget, part_value, part_gate, total = sent_together(
        (
            part_query.astype(jnp.bfloat16),
            part_forget.astype(jnp.bfloat16),
            part_value.astype(jnp.bfloat16),
            part_gate.astype(jnp.bfloat16),
            squares.astype(jnp.bfloat16),
        ),
        "kv",
        0,
        1,
    )
    inverse = lax.rsqrt(total / D + EPS)[:, None]
    bound = lower_bound.reshape(local_heads, DK)
    forget_raw = (part_forget * inverse).reshape(local_seqs, local_heads, DK)
    forget = bound + (1.0 - bound) * jax.nn.sigmoid(forget_raw)
    keyvec = (1.0 - bound) * jax.nn.sigmoid(-forget_raw)
    query = jax.nn.silu((part_query * inverse).reshape(local_seqs, local_heads, DK))
    values = (part_value * inverse).reshape(local_seqs, local_heads, DV)
    updated = forget[..., None] * state + keyvec[..., None] * values[:, :, None, :]
    head_out = jnp.einsum("shc,shce->she", query, updated, precision=lax.Precision.HIGHEST)
    inv_head = lax.rsqrt(jnp.mean(head_out * head_out, axis=2, keepdims=True) + EPS)
    out_gate = jax.nn.silu((part_gate * inverse).reshape(local_seqs, local_heads, DV))
    normed = (
        (head_out * inv_head * head_gain * out_gate)
        .reshape(local_seqs, local_heads * DV)
        .astype(jnp.bfloat16)
    )
    terms = project_row(w_mix_out, collect(normed, "kv", 0))
    mixed = nested_sum(terms, "tp")
    after_mix = (rows_float + mixed).astype(jnp.bfloat16)
    layer_out = channel_mix(after_mix, ffn_gain, w_gate, w_up, w_down)
    return (layer_out, updated)


def solution(mesh):
    in_specs = (
        P(None, ("kv", "tp")),
        P("kv"),
        P("kv", "tp"),
        P("kv", "tp"),
        P("kv", "tp"),
        P("kv", "tp"),
        P("tp"),
        P("kv", "tp", None, None),
        P(),
        P("tp", "kv"),
        P("kv"),
        P("kv", "tp"),
        P("kv", "tp"),
        P("tp", "kv"),
    )
    out_specs = (P(None, ("kv", "tp")), P("kv", "tp", None, None))
    return jax.shard_map(body, mesh=mesh, in_specs=in_specs, out_specs=out_specs, check_vma=False)
```

profile of v0, /device:TPU:25, one launch (start us, length us, event | category | flops | bytes accessed | tf_op | source)
XLA Modules:
  0.0 262.5 jit_solution(13635138778314057084)
XLA Ops:
  1.5 38.0 %all_to_all.74 = bf16[32,512,8]{1,2,0:T(8,128)(2,1)S(1)} all-to-all(bf16[32,512,8]{1,2,0:T(8,128)(2,1)S(1)} %broadcast_in_dim.12), channel_id=1, replica_groups=mesh['kv'=16,'tp'=32] {'tp'}, dimensions={0} | all-to-all | bytes 524288 | tf_op jit(solution)/shard_map/all_to_all | solution.py:31
  46.3 6.6 %all-to-all-start.1 = ((bf16[16,32,513]{2,1,0:T(8,128)(2,1)}), bf16[16,32,513]{2,1,0:T(8,128)(2,1)S(1)}, u32[]{:S(2)}, u32[]{:S(2)}) async-start(bf16[16,32,513]{2,1,0:T(8,128)(2,1)} %constant_dynamic-update-slice_fusion), calls=%async_computation.1 | async-start | bytes 1310720 | tf_op jit(solution)/shard_map/all_to_all | solution.py:46
  52.9 10.0 %all-to-all-done.1 = bf16[16,32,513]{2,1,0:T(8,128)(2,1)S(1)} async-done(((bf16[16,32,513]{2,1,0:T(8,128)(2,1)}), bf16[16,32,513]{2,1,0:T(8,128)(2,1)S(1)}, u32[]{:S(2)}, u32[]{:S(2)}) %all-to-all-start.1) | async-done | bytes 525344 | tf_op jit(solution)/shard_map/all_to_all | solution.py:46
  63.3 2.5 multiply_add_fusion
  67.9 10.4 %all_to_all.75 = bf16[16,32,128]{2,1,0:T(8,128)(2,1)S(1)} all-to-all(bf16[16,32,128]{2,1,0:T(8,128)(2,1)S(1)} %broadcast_in_dim.13), channel_id=1, replica_groups=mesh['kv'=16,'tp'=32] {'kv'}, dimensions={0} | all-to-all | bytes 262144 | tf_op jit(solution)/shard_map/all_to_all | solution.py:31
  78.5 38.7 %all_to_all.76 = f32[32,16,256]{2,1,0:T(8,128)S(1)} all-to-all(f32[32,16,256]{2,1,0:T(8,128)S(1)} %fusion.9), channel_id=1, replica_groups=mesh['kv'=16,'tp'=32] {'tp'}, dimensions={0} | all-to-all | bytes 1048576 | tf_op jit(solution)/shard_map/all_to_all | solution.py:71
  118.1 4.3 %all-to-all-start.4 = ((f32[32,16,256]{2,1,0:T(8,128)}), f32[32,16,256]{2,1,0:T(8,128)S(1)}, u32[]{:S(2)}, u32[]{:S(2)}) async-start(f32[32,16,256]{2,1,0:T(8,128)} %broadcast_in_dim.14), calls=%async_computation.4 | async-start | bytes 1048576 | tf_op jit(solution)/shard_map/all_to_all | solution.py:31
  122.5 2.8 %reshape.179 = f32[32,16,256]{1,0,2:T(8,128)} reshape(f32[512,32,8]{0,2,1:T(8,128)S(1)} %convert_bitcast_fusion.1) | data formatting | bytes 1048576 | tf_op jit(solution)/shard_map/convert_element_type | solution.py:124
  125.2 3.5 %copy.67 = f32[32,16,256]{2,1,0:T(8,128)S(1)} copy(f32[32,16,256]{1,0,2:T(8,128)} %reshape.179) | data formatting | bytes 1048576 | tf_op jit(solution)/shard_map/convert_element_type | solution.py:124
  128.7 27.2 %all-to-all-done.4 = f32[32,16,256]{2,1,0:T(8,128)S(1)} async-done(((f32[32,16,256]{2,1,0:T(8,128)}), f32[32,16,256]{2,1,0:T(8,128)S(1)}, u32[]{:S(2)}, u32[]{:S(2)}) %all-to-all-start.4) | async-done | bytes 524320 | tf_op jit(solution)/shard_map/all_to_all | solution.py:31
  157.0 5.4 %all-to-all-start.7 = ((bf16[16,1,32]{2,1,0:T(2,128)(2,1)}), bf16[16,1,32]{2,1,0:T(2,128)(2,1)S(1)}, u32[]{:S(2)}, u32[]{:S(2)}) async-start(bf16[16,1,32]{2,1,0:T(2,128)(2,1)} %convert_element_type.168), calls=%async_computation.7 | async-start | bytes 16384 | tf_op jit(solution)/shard_map/all_to_all | solution.py:46
  162.4 4.5 %all-to-all-done.7 = bf16[16,1,32]{2,1,0:T(2,128)(2,1)S(1)} async-done(((bf16[16,1,32]{2,1,0:T(2,128)(2,1)}), bf16[16,1,32]{2,1,0:T(2,128)(2,1)S(1)}, u32[]{:S(2)}, u32[]{:S(2)}) %all-to-all-start.7) | async-done | bytes 1056 | tf_op jit(solution)/shard_map/all_to_all | solution.py:46
  167.6 5.1 %all-to-all-start.8 = ((bf16[16,1,32]{2,1,0:T(2,128)(2,1)}), bf16[16,1,32]{2,1,0:T(2,128)(2,1)S(1)}, u32[]{:S(2)}, u32[]{:S(2)}) async-start(bf16[16,1,32]{2,1,0:T(2,128)(2,1)} %broadcast_in_dim.32), calls=%async_computation.8 | async-start | bytes 16384 | tf_op jit(solution)/shard_map/all_to_all | solution.py:31
  174.7 2.8 %reduce.19 = bf16[16,10752]{1,0:T(8,128)(2,1)S(1)} reduce(bf16[16,1,10752]{2,1,0:T(2,128)(2,1)S(1)} %all_to_all.60, bf16[]{:T(256)} %broadcast.95), dimensions={1}, to_apply=%all_to_all.60.reduce_sub_computation | reduce | bytes 688130 | tf_op jit(solution)/shard_map/all_to_all | solution.py:46
  178.2 6.7 %all-to-all-start.5 = ((bf16[16,2,5376]{2,1,0:T(2,128)(2,1)}), bf16[16,2,5376]{2,1,0:T(2,128)(2,1)S(1)}, u32[]{:S(2)}, u32[]{:S(2)}) async-start(bf16[16,2,5376]{2,1,0:T(2,128)(2,1)} %reshape.191), calls=%async_computation.5 | async-start | bytes 688128 | tf_op jit(solution)/shard_map/all_to_all | solution.py:46
  186.2 2.8 %reduce.17 = bf16[16,10752]{1,0:T(8,128)(2,1)S(1)} reduce(bf16[16,1,10752]{2,1,0:T(2,128)(2,1)S(1)} %all_to_all.61, bf16[]{:T(256)} %broadcast.95), dimensions={1}, to_apply=%all_to_all.61.reduce_sub_computation | reduce | bytes 688130 | tf_op jit(solution)/shard_map/all_to_all | solution.py:46
  190.9 5.6 %all-to-all-start.9 = ((bf16[16,2,5376]{2,1,0:T(2,128)(2,1)}), bf16[16,2,5376]{2,1,0:T(2,128)(2,1)S(1)}, u32[]{:S(2)}, u32[]{:S(2)}) async-start(bf16[16,2,5376]{2,1,0:T(2,128)(2,1)} %reshape.187), calls=%async_computation.9 | async-start | bytes 688128 | tf_op jit(solution)/shard_map/all_to_all | solution.py:46
  197.8 2.8 %reduce.20 = bf16[16,10752]{1,0:T(8,128)(2,1)S(1)} reduce(bf16[16,1,10752]{2,1,0:T(2,128)(2,1)S(1)} %broadcast_in_dim.15, bf16[]{:T(256)} %broadcast.95), dimensions={1}, to_apply=%broadcast_in_dim.15.reduce_sub_computation | reduce | bytes 688130 | tf_op jit(solution)/shard_map/broadcast_in_dim | solution.py:30
  202.5 5.5 %all-to-all-start.6 = ((bf16[16,2,5376]{2,1,0:T(2,128)(2,1)}), bf16[16,2,5376]{2,1,0:T(2,128)(2,1)S(1)}, u32[]{:S(2)}, u32[]{:S(2)}) async-start(bf16[16,2,5376]{2,1,0:T(2,128)(2,1)} %reshape.193), calls=%async_computation.6 | async-start | bytes 688128 | tf_op jit(solution)/shard_map/all_to_all | solution.py:31
  209.3 2.8 %reduce.18 = bf16[16,10752]{1,0:T(8,128)(2,1)S(1)} reduce(bf16[16,1,10752]{2,1,0:T(2,128)(2,1)S(1)} %broadcast_in_dim.33, bf16[]{:T(256)} %broadcast.95), dimensions={1}, to_apply=%broadcast_in_dim.33.reduce_sub_computation | reduce | bytes 688130 | tf_op jit(solution)/shard_map/broadcast_in_dim | solution.py:30
  214.0 5.6 %all-to-all-start.10 = ((bf16[16,2,5376]{2,1,0:T(2,128)(2,1)}), bf16[16,2,5376]{2,1,0:T(2,128)(2,1)S(1)}, u32[]{:S(2)}, u32[]{:S(2)}) async-start(bf16[16,2,5376]{2,1,0:T(2,128)(2,1)} %reshape.189), calls=%async_computation.10 | async-start | bytes 688128 | tf_op jit(solution)/shard_map/all_to_all | solution.py:31
  222.7 2.9 %all-to-all-done.10 = bf16[16,2,5376]{2,1,0:T(2,128)(2,1)S(1)} async-done(((bf16[16,2,5376]{2,1,0:T(2,128)(2,1)}), bf16[16,2,5376]{2,1,0:T(2,128)(2,1)S(1)}, u32[]{:S(2)}, u32[]{:S(2)}) %all-to-all-start.10) | async-done | bytes 344096 | tf_op jit(solution)/shard_map/all_to_all | solution.py:31
  229.8 10.4 %all-to-all-start.11 = ((bf16[32,512,8]{1,2,0:T(8,128)(2,1)}), bf16[32,512,8]{1,2,0:T(8,128)(2,1)S(1)}, u32[]{:S(2)}, u32[]{:S(2)}) async-start(bf16[32,512,8]{1,2,0:T(8,128)(2,1)} %fusion.2), calls=%async_computation.11 | async-start | bytes 524288 | tf_op jit(solution)/shard_map/all_to_all | solution.py:46
  240.2 21.6 %all-to-all-done.11 = bf16[32,512,8]{1,2,0:T(8,128)(2,1)S(1)} async-done(((bf16[32,512,8]{1,2,0:T(8,128)(2,1)}), bf16[32,512,8]{1,2,0:T(8,128)(2,1)S(1)}, u32[]{:S(2)}, u32[]{:S(2)}) %all-to-all-start.11) | async-done | bytes 262176 | tf_op jit(solution)/shard_map/all_to_all | solution.py:46
  (85 shorter events, 33.3 us)
Async XLA Ops:
  0.6 172.2 %copy-start = (bf16[256,336]{0,1:T(8,128)(2,1)S(1)}, bf16[256,336]{0,1:T(8,128)(2,1)}, u32[]{:S(2)}) copy-start(bf16[256,336]{0,1:T(8,128)(2,1)} %param.25) | copy-start | bytes 516100
  0.6 42.9 %copy-start.6 = (f32[256]{0:T(256)S(1)}, f32[256]{0:T(256)}, u32[]{:S(2)}) copy-start(f32[256]{0:T(256)} %param.15) | copy-start | bytes 3076
  0.7 42.9 %copy-start.3 = (bf16[256,128]{1,0:T(8,128)(2,1)S(1)}, bf16[256,128]{1,0:T(8,128)(2,1)}, u32[]{:S(2)}) copy-start(bf16[256,128]{1,0:T(8,128)(2,1)} %param.18) | copy-start | bytes 196612
  0.7 43.9 %copy-start.4 = (bf16[256,128]{1,0:T(8,128)(2,1)S(1)}, bf16[256,128]{1,0:T(8,128)(2,1)}, u32[]{:S(2)}) copy-start(bf16[256,128]{1,0:T(8,128)(2,1)} %param.19) | copy-start | bytes 196612
  41.3 11.6 %copy-start.8 = (f32[128]{0:T(128)S(1)}, f32[128]{0:T(128)}, u32[]{:S(2)}) copy-start(f32[128]{0:T(128)} %param.20) | copy-start | bytes 1540
  46.3 16.7 %all-to-all-start.1 = ((bf16[16,32,513]{2,1,0:T(8,128)(2,1)}), bf16[16,32,513]{2,1,0:T(8,128)(2,1)S(1)}, u32[]{:S(2)}, u32[]{:S(2)}) async-start(bf16[16,32,513]{2,1,0:T(8,128)(2,1)} %constant_dynamic-update-slice_fusion), calls=%async_computation.1 | async-start | bytes 1310720 | tf_op jit(solution)/shard_map/all_to_all | solution.py:46
  65.7 51.4 %copy-start.1 = (f32[32,1,128,128]{3,2,1,0:T(8,128)}, f32[32,1,128,128]{3,2,1,0:T(8,128)S(1)}, u32[]{:S(2)}) copy-start(f32[32,1,128,128]{3,2,1,0:T(8,128)S(1)} %multiply_add_fusion) | copy-start | bytes 6291460
  65.7 2.0 copy-start.9
  65.8 12.5 %copy-start.5 = (bf16[128,256]{1,0:T(8,128)(2,1)S(1)}, bf16[128,256]{1,0:T(8,128)(2,1)}, u32[]{:S(2)}) copy-start(bf16[128,256]{1,0:T(8,128)(2,1)} %param.23) | copy-start | bytes 196612
  118.1 37.9 %all-to-all-start.4 = ((f32[32,16,256]{2,1,0:T(8,128)}), f32[32,16,256]{2,1,0:T(8,128)S(1)}, u32[]{:S(2)}, u32[]{:S(2)}) async-start(f32[32,16,256]{2,1,0:T(8,128)} %broadcast_in_dim.14), calls=%async_computation.4 | async-start | bytes 1048576 | tf_op jit(solution)/shard_map/all_to_all | solution.py:31
  128.7 44.1 %copy-start.7 = (f32[256]{0:T(256)S(1)}, f32[256]{0:T(256)}, u32[]{:S(2)}) copy-start(f32[256]{0:T(256)} %param.24) | copy-start | bytes 3076
  157.0 10.0 %all-to-all-start.7 = ((bf16[16,1,32]{2,1,0:T(2,128)(2,1)}), bf16[16,1,32]{2,1,0:T(2,128)(2,1)S(1)}, u32[]{:S(2)}, u32[]{:S(2)}) async-start(bf16[16,1,32]{2,1,0:T(2,128)(2,1)} %convert_element_type.168), calls=%async_computation.7 | async-start | bytes 16384 | tf_op jit(solution)/shard_map/all_to_all | solution.py:46
  167.6 10.6 %all-to-all-start.8 = ((bf16[16,1,32]{2,1,0:T(2,128)(2,1)}), bf16[16,1,32]{2,1,0:T(2,128)(2,1)S(1)}, u32[]{:S(2)}, u32[]{:S(2)}) async-start(bf16[16,1,32]{2,1,0:T(2,128)(2,1)} %broadcast_in_dim.32), calls=%async_computation.8 | async-start | bytes 16384 | tf_op jit(solution)/shard_map/all_to_all | solution.py:31
  173.1 11.8 %copy-start.2 = (bf16[256,336]{0,1:T(8,128)(2,1)S(1)}, bf16[256,336]{0,1:T(8,128)(2,1)}, u32[]{:S(2)}) copy-start(bf16[256,336]{0,1:T(8,128)(2,1)} %param.26) | copy-start | bytes 516100
  178.2 12.6 %all-to-all-start.5 = ((bf16[16,2,5376]{2,1,0:T(2,128)(2,1)}), bf16[16,2,5376]{2,1,0:T(2,128)(2,1)S(1)}, u32[]{:S(2)}, u32[]{:S(2)}) async-start(bf16[16,2,5376]{2,1,0:T(2,128)(2,1)} %reshape.191), calls=%async_computation.5 | async-start | bytes 688128 | tf_op jit(solution)/shard_map/all_to_all | solution.py:46
  190.9 11.7 %all-to-all-start.9 = ((bf16[16,2,5376]{2,1,0:T(2,128)(2,1)}), bf16[16,2,5376]{2,1,0:T(2,128)(2,1)S(1)}, u32[]{:S(2)}, u32[]{:S(2)}) async-start(bf16[16,2,5376]{2,1,0:T(2,128)(2,1)} %reshape.187), calls=%async_computation.9 | async-start | bytes 688128 | tf_op jit(solution)/shard_map/all_to_all | solution.py:46
  202.5 11.4 %all-to-all-start.6 = ((bf16[16,2,5376]{2,1,0:T(2,128)(2,1)}), bf16[16,2,5376]{2,1,0:T(2,128)(2,1)S(1)}, u32[]{:S(2)}, u32[]{:S(2)}) async-start(bf16[16,2,5376]{2,1,0:T(2,128)(2,1)} %reshape.193), calls=%async_computation.6 | async-start | bytes 688128 | tf_op jit(solution)/shard_map/all_to_all | solution.py:31
  214.0 11.6 %all-to-all-start.10 = ((bf16[16,2,5376]{2,1,0:T(2,128)(2,1)}), bf16[16,2,5376]{2,1,0:T(2,128)(2,1)S(1)}, u32[]{:S(2)}, u32[]{:S(2)}) async-start(bf16[16,2,5376]{2,1,0:T(2,128)(2,1)} %reshape.189), calls=%async_computation.10 | async-start | bytes 688128 | tf_op jit(solution)/shard_map/all_to_all | solution.py:31
  222.6 5.9 %copy-start.10 = (bf16[336,256]{1,0:T(8,128)(2,1)S(1)}, bf16[336,256]{1,0:T(8,128)(2,1)}, u32[]{:S(2)}) copy-start(bf16[336,256]{1,0:T(8,128)(2,1)} %param.27) | copy-start | bytes 516100
  229.8 32.1 %all-to-all-start.11 = ((bf16[32,512,8]{1,2,0:T(8,128)(2,1)}), bf16[32,512,8]{1,2,0:T(8,128)(2,1)S(1)}, u32[]{:S(2)}, u32[]{:S(2)}) async-start(bf16[32,512,8]{1,2,0:T(8,128)(2,1)} %fusion.2), calls=%async_computation.11 | async-start | bytes 524288 | tf_op jit(solution)/shard_map/all_to_all | solution.py:46
where the time goes:
time: 267 us; the launch traced here: 263 us
  blocking collectives  87 us (33%)
  waiting for transfers between devices  69.6 us (26%)
  starting transfers between devices  55.2 us (21%)
  local copies, waits for them, and re-layouts  22.1 us (8%)
  other arithmetic  20.5 us (8%)
  matrix products  7.1 us (3%)
    all_to_all x2, blocking collectives, copy_for_each(): return lax.all_to_all(copies, axis, split_axis=0, concat_axis=0, tiled=True)  48.3 us
    all_to_all x1, blocking collectives, summed_on_arrival_2(): tiles = lax.all_to_all(cut_along(shard, dim, size), axis, 0, 0, tiled=True)  38.7 us
    all_to_all x5, waiting for transfers between devices, summed_on_arrival(): lax.all_to_all(tiles, axis, split_axis=0, concat_axis=0, tiled=True)  38.5 us
    all_to_all x5, starting transfers between devices, summed_on_arrival(): lax.all_to_all(tiles, axis, split_axis=0, concat_axis=0, tiled=True)  34.7 us
    all_to_all x4, waiting for transfers between devices, copy_for_each(): return lax.all_to_all(copies, axis, split_axis=0, concat_axis=0, tiled=True)  31.1 us
    all_to_all x4, starting transfers between devices, copy_for_each(): return lax.all_to_all(copies, axis, split_axis=0, concat_axis=0, tiled=True)  20.5 us
    unnamed x34, local copies, waits for them, and re-layouts  7.09 us
    convert_element_type x2, local copies, waits for them, and re-layouts, body(): rows_float = rows.astype(jnp.float32)  6.27 us
  transfers between devices with their start and end apart: 9, of which 8 were waited for; matrix products, arithmetic and copies ran while one was open for 11% of the time, Pallas kernels for 0%

commit v1 on v0

v1 whole, which is shorter than its diff:
```python
import functools

import jax
import jax.numpy as jnp
from jax import lax
from jax.experimental import pallas as pl
from jax.experimental.pallas import tpu as pltpu
from jax.sharding import PartitionSpec as P

D = 4096
EPS = 1e-06
KV = 16
Z = 16
SEQ = 512
LOC = 32
F = 256
FFL = 336
FFP = 384
MESH = pl.DeviceIdType.MESH
NT = (((1,), (1,)), ((), ()))
f32 = jnp.float32
bf16 = jnp.bfloat16


def sigmoid(u):
    return 1.0 / (1.0 + jnp.exp(-u))


def silu(u):
    return u * sigmoid(u)


def z_step(j):
    sign = 1 - 2 * lax.rem(j, 2)
    return 8 + sign * ((j + 1) // 2)


def layer_kernel(
    x_ref, mg_ref, lb_ref, hg_ref, fg_ref,
    wq_hbm, wf_hbm, wi_hbm, wo_hbm, state_hbm, wm_hbm, wg_hbm, wu_hbm, wd_hbm,
    out_ref, ns_hbm,
    wp, wm, wg, wu, wd, st, ns,
    x1, s2, sq2, r2, rq2, qt, ft, kt, vals, ho, n3, t4, p4, d4, s4, r4, own5, x5,
    s6, r6, h7, hw7, t8, p8, d8, s8, r8,
    wsem, stsem, nssem, loc,
    s1s, r1s, f1s, f1r, s2s, r2s, q2s, q2r, s3s, r3s, d4s, d4r, s4s, r4s,
    s5s, r5s, f5s, f5r, s6s, r6s, s7s, r7s, d8s, d8r, s8s, r8s,
):
    k = lax.axis_index("kv")
    t = lax.axis_index("tp")
    z = t // 2
    c = lax.rem(t, 2)
    o = 1 - c
    ky = k // 4
    kx = lax.rem(k, 4)
    mate = 2 * z + o

    def kv_to(r):
        return lax.rem(ky + r // 4, 4) * 4 + lax.rem(kx + lax.rem(r, 4), 4)

    def z_to(r):
        return lax.rem(z + r, Z)

    def z_from(r):
        return lax.rem(z - r + Z, Z)

    def rcopy(src, dst, ssem, rsem, kk, tt):
        return pltpu.make_async_remote_copy(
            src_ref=src, dst_ref=dst, send_sem=ssem, recv_sem=rsem,
            device_id=(kk, tt), device_id_type=MESH,
        )

    def all_sent(view, ssem, rsem):
        rcopy(view, view, ssem, rsem, k, mate).wait_send()

    def all_here(view, ssem, rsem):
        rcopy(view, view, ssem, rsem, k, mate).wait_recv()

    loads = [
        pltpu.make_async_copy(src, dst, wsem.at[i])
        for i, (src, dst) in enumerate(
            (
                (wq_hbm, wp.at[0]), (wf_hbm, wp.at[1]), (wi_hbm, wp.at[2]), (wo_hbm, wp.at[3]),
                (wm_hbm, wm), (wg_hbm, wg), (wu_hbm, wu), (wd_hbm, wd),
            )
        )
    ]
    for load in loads:
        load.start()
    state_in = pltpu.make_async_copy(state_hbm, st, stsem)
    state_in.start()

    barrier = pltpu.get_barrier_semaphore()

    def greet_z(j, _):
        pl.semaphore_signal(barrier, inc=1, device_id=(k, 2 * z_to(z_step(j)) + c), device_id_type=MESH)
        return 0

    def greet_kv(r, _):
        pl.semaphore_signal(barrier, inc=1, device_id=(kv_to(r), t), device_id_type=MESH)
        return 0

    lax.fori_loop(0, Z - 1, greet_z, 0)
    lax.fori_loop(1, KV, greet_kv, 0)
    pl.semaphore_signal(barrier, inc=1, device_id=(k, mate), device_id_type=MESH)
    pl.semaphore_wait(barrier, (Z - 1) + (KV - 1) + 1)

    def gather_tp(own, slots, ss, rs, fs, fr):
        def send(j, _):
            r = z_step(j)
            rcopy(own, slots.at[t], ss, rs.at[r], k, 2 * z_to(r) + c).start()
            return 0

        lax.fori_loop(0, Z - 1, send, 0)
        rcopy(own, slots.at[t], fs, fr, k, mate).start()

        def forward(i, _):
            r = z_step(Z - 2 - i)
            src = 2 * z_from(r) + c
            rcopy(own, slots.at[src], ss, rs.at[r], k, mate).wait_recv()
            rcopy(slots.at[src], slots.at[src], fs, fr, k, mate).start()
            return 0

        lax.fori_loop(0, Z - 1, forward, 0)
        all_here(slots.at[pl.ds(0, Z)], fs, fr)

    x1[t] = x_ref[...]
    gather_tp(x_ref, x1, s1s, r1s, f1s, f1r)

    xt = x1[...].astype(f32).reshape(F, SEQ)
    row = jnp.sum(xt * xt, axis=0, keepdims=True)
    for i in range(4):
        sq2[i : i + 1, :] = row[:, 128 * i : 128 * i + 128]
        sq2[4 + i : 5 + i, :] = row[:, 128 * i : 128 * i + 128]
    xf = xt.T
    scaled = (xf * mg_ref[...]).astype(bf16)
    for i in range(4):
        loads[i].wait()
        part = jnp.dot(scaled, wp[i], preferred_element_type=f32)
        s2[:, :, 128 * i : 128 * i + 128] = part.astype(bf16).reshape(KV, LOC, 128)

    def send2(r, _):
        kk = kv_to(r)
        rcopy(s2.at[kk], r2.at[r - 1], s2s, r2s, kk, t).start()
        rcopy(sq2, rq2.at[r - 1], q2s, q2r, kk, t).start()
        return 0

    lax.fori_loop(1, KV, send2, 0)
    state_in.wait()
    all_here(rq2, q2s, q2r)
    all_here(r2, s2s, r2s)

    sq = sq2[...]
    raw = s2[k].astype(f32)
    for i in range(KV - 1):
        sq = sq + rq2[i]
        raw = raw + r2[i].astype(f32)
    tile_row = lax.broadcasted_iota(jnp.int32, (8, 128), 0)
    line = jnp.sum(jnp.where(tile_row == ky, sq, 0.0), axis=0, keepdims=True)
    lane = lax.broadcasted_iota(jnp.int32, (LOC, 128), 1)
    seq = lax.broadcasted_iota(jnp.int32, (LOC, 128), 0)
    total = jnp.sum(jnp.where(lane == seq + kx * LOC, line, 0.0), axis=1, keepdims=True)
    raw = raw * lax.rsqrt(total / D + EPS)

    bound = lb_ref[...]
    forget_raw = raw[:, 128:256]
    forget = bound + (1.0 - bound) * sigmoid(forget_raw)
    keyvec = (1.0 - bound) * sigmoid(-forget_raw)
    query = silu(raw[:, 0:128])
    vals[...] = raw[:, 256:384]
    out_gate = silu(raw[:, 384:512])
    fill = jnp.zeros((128 - LOC, 128), f32)
    qt[...] = jnp.concatenate([query, fill], axis=0).T
    ft[...] = jnp.concatenate([forget, fill], axis=0).T
    kt[...] = jnp.concatenate([keyvec, fill], axis=0).T
    lanes = lax.broadcasted_iota(jnp.int32, (128, 128), 1)

    def recur(s, _):
        here = lanes == s

        def column(ref):
            return jnp.sum(jnp.where(here, ref[...], 0.0), axis=1, keepdims=True)

        new = column(ft) * st[s] + column(kt) * vals[pl.ds(s, 1), :]
        ns[s] = new
        ho[pl.ds(s, 1), :] = jnp.sum(column(qt) * new, axis=0, keepdims=True)
        return 0

    lax.fori_loop(0, LOC, recur, 0)
    state_out = pltpu.make_async_copy(ns, ns_hbm, nssem)
    state_out.start()

    head = ho[...]
    inv = lax.rsqrt(jnp.mean(head * head, axis=1, keepdims=True) + EPS)
    own3 = (head * inv * hg_ref[...] * out_gate).astype(bf16)

    n3[k] = own3

    def send3(r, _):
        rcopy(n3.at[k], n3.at[k], s3s, r3s, kv_to(r), t).start()
        return 0

    lax.fori_loop(1, KV, send3, 0)
    loads[4].wait()
    all_here(n3.at[pl.ds(0, KV - 1)], s3s, r3s)

    mixed = jnp.dot(n3[...].reshape(SEQ, 128), wm[...], preferred_element_type=f32)
    for b in range(2 * Z):
        t4[b % 2, b // 2] = mixed[16 * b : 16 * b + 16, :]

    def sum_tp(terms, pairs, got, ring, land, ds_, dr_, ss, rs):
        pairs[...] = terms[o].astype(bf16)
        swap = rcopy(pairs, got, ds_, dr_, k, mate)
        swap.start()
        swap.wait_recv()
        both = terms[c] + got[...].astype(f32)
        ring[...] = both.astype(bf16)
        terms[c] = both

        def send(j, _):
            r = z_step(j)
            zz = z_to(r)
            rcopy(ring.at[zz], land.at[r - 1], ss, rs, k, 2 * zz + c).start()
            return 0

        lax.fori_loop(0, Z - 1, send, 0)
        all_here(land, ss, rs)
        total_ = terms[c, z]
        for i in range(Z - 1):
            total_ = total_ + land[i].astype(f32)
        return total_

    summed = sum_tp(t4, p4, d4, s4, r4, d4s, d4r, s4s, r4s)
    hw7[...] = xf
    mine = hw7[pl.ds(pl.multiple_of(t * 16, 16), 16), :]
    own5[...] = (mine + summed).astype(bf16)
    x5[t] = own5[...]
    gather_tp(own5, x5, s5s, r5s, f5s, f5r)

    after = x5[...].reshape(SEQ, F).astype(f32)
    squares = jnp.sum(after * after, axis=1, keepdims=True)
    scaled = (after * fg_ref[...]).astype(bf16)
    loads[5].wait()
    gate = lax.dot_general(scaled, wg[...], NT, preferred_element_type=f32)
    s6[:, :, 0:FFL] = gate.astype(bf16).reshape(KV, LOC, FFL)
    loads[6].wait()
    upper = lax.dot_general(scaled, wu[...], NT, preferred_element_type=f32)
    s6[:, :, FFP : FFP + FFL] = upper.astype(bf16).reshape(KV, LOC, FFL)
    high = squares.astype(bf16)
    low = (squares - high.astype(f32)).astype(bf16)
    spot = lax.broadcasted_iota(jnp.int32, (SEQ, FFP - FFL), 1)
    tail = jnp.where(spot == 0, high.astype(f32), jnp.where(spot == 1, low.astype(f32), 0.0))
    s6[:, :, FFL:FFP] = tail.astype(bf16).reshape(KV, LOC, FFP - FFL)
    s6[:, :, FFP + FFL : 2 * FFP] = jnp.zeros((KV, LOC, FFP - FFL), bf16)

    def send6(r, _):
        kk = kv_to(r)
        rcopy(s6.at[kk], r6.at[r - 1], s6s, r6s, kk, t).start()
        return 0

    lax.fori_loop(1, KV, send6, 0)
    hw7[...] = after
    own_t = hw7[...].T
    loads[7].wait()
    all_here(r6, s6s, r6s)
    both = s6[k].astype(f32)
    for i in range(KV - 1):
        both = both + r6[i].astype(f32)
    total = both[:, FFL : FFL + 1] + both[:, FFL + 1 : FFL + 2]
    inverse = lax.rsqrt(total / D + EPS)
    hidden = silu(both[:, 0:FFP] * inverse) * (both[:, FFP : 2 * FFP] * inverse)
    spot = lax.broadcasted_iota(jnp.int32, (LOC, FFP), 1)
    h7[k] = jnp.where(spot < FFL, hidden, 0.0).astype(bf16)

    def send7(r, _):
        rcopy(h7.at[k], h7.at[k], s7s, r7s, kv_to(r), t).start()
        return 0

    lax.fori_loop(1, KV, send7, 0)
    t8[...] = own_t.reshape(2 * Z, 8, SEQ)
    own8 = t8[t]
    all_here(h7.at[pl.ds(0, KV - 1)], s7s, r7s)
    hall = h7[...].reshape(SEQ, FFP)
    down = jnp.dot(hall[:, 0:FFL], wd[...], preferred_element_type=f32)
    down = down.T
    for b in range(2 * Z):
        p = down[8 * b : 8 * b + 8, :]
        d = b
        t8[(d % 2) * Z + d // 2] = p

    summed = sum_tp8(t8, p8, d8, s8, r8, d8s, d8r, s8s, r8s, c, o, z, k, mate, rcopy, all_here, z_to)
    out_ref[...] = (own8 + summed).astype(bf16)

    slots = x1.at[pl.ds(0, Z - 1)]
    all_sent(slots, s1s, r1s.at[0])
    all_sent(x1.at[pl.ds(0, Z)], f1s, f1r)
    all_sent(r2, s2s, r2s)
    all_sent(rq2, q2s, q2r)
    all_sent(n3.at[pl.ds(0, KV - 1)], s3s, r3s)
    all_sent(p4, d4s, d4r)
    all_sent(r4, s4s, r4s)
    all_sent(x5.at[pl.ds(0, Z - 1)], s5s, r5s.at[0])
    all_sent(x5.at[pl.ds(0, Z)], f5s, f5r)
    all_sent(r6, s6s, r6s)
    all_sent(h7.at[pl.ds(0, KV - 1)], s7s, r7s)
    all_sent(p8, d8s, d8r)
    all_sent(r8, s8s, r8s)
    state_out.wait()


def sum_tp8(terms, pairs, got, ring, land, ds_, dr_, ss, rs, c, o, z, k, mate, rcopy, all_here, z_to):
    pairs[...] = terms[pl.ds(o * Z, Z)].astype(bf16)
    swap = rcopy(pairs, got, ds_, dr_, k, mate)
    swap.start()
    swap.wait_recv()
    both = terms[pl.ds(c * Z, Z)] + got[...].astype(f32)
    ring[...] = both.astype(bf16)
    terms[pl.ds(c * Z, Z)] = both

    def send(j, _):
        r = z_step(j)
        zz = z_to(r)
        rcopy(ring.at[zz], land.at[r - 1], ss, rs, k, 2 * zz + c).start()
        return 0

    lax.fori_loop(0, Z - 1, send, 0)
    all_here(land, ss, rs)
    total = terms[c * Z + z]
    for i in range(Z - 1):
        total = total + land[i].astype(f32)
    return total


def body(
    residual, mixer_gain, w_query, w_forget, w_input, w_outgate, lower_bound, state, head_gain,
    w_mix_out, ffn_gain, w_gate, w_up, w_down,
):
    vmem = pl.BlockSpec(memory_space=pltpu.VMEM)
    hbm = pl.BlockSpec(memory_space=pl.ANY)
    V = pltpu.VMEM
    dma = pltpu.SemaphoreType.DMA
    scratch = [
        V((4, F, 128), bf16), V((128, F), bf16), V((FFL, F), bf16), V((FFL, F), bf16), V((FFL, F), bf16),
        V((LOC, 128, 128), f32), V((LOC, 128, 128), f32),
        V((2 * Z, 8, SEQ), bf16),
        V((KV, LOC, 512), bf16), V((8, 128), f32), V((KV - 1, LOC, 512), bf16), V((KV - 1, 8, 128), f32),
        V((128, 128), f32), V((128, 128), f32), V((128, 128), f32), V((LOC, 128), f32), V((LOC, 128), f32),
        V((KV, LOC, 128), bf16),
        V((2, Z, 16, F), f32), V((Z, 16, F), bf16), V((Z, 16, F), bf16), V((Z, 16, F), bf16), V((Z - 1, 16, F), bf16),
        V((16, F), bf16), V((2 * Z, 16, F), bf16),
        V((KV, LOC, 2 * FFP), bf16), V((KV - 1, LOC, 2 * FFP), bf16), V((KV, LOC, FFP), bf16), V((SEQ, F), f32),
        V((2 * Z, 8, SEQ), f32), V((Z, 8, SEQ), bf16), V((Z, 8, SEQ), bf16), V((Z, 8, SEQ), bf16), V((Z - 1, 8, SEQ), bf16),
        dma((8,)), dma, dma, dma,
        dma, dma((Z,)), dma, dma, dma, dma, dma, dma, dma, dma, dma, dma, dma, dma,
        dma, dma((Z,)), dma, dma, dma, dma, dma, dma, dma, dma, dma, dma,
    ]
    out, new_state = pl.pallas_call(
        layer_kernel,
        out_shape=(
            jax.ShapeDtypeStruct((8, SEQ), bf16),
            jax.ShapeDtypeStruct((LOC, 128, 128), f32),
        ),
        in_specs=[vmem] * 5 + [hbm] * 9,
        out_specs=(vmem, hbm),
        scratch_shapes=scratch,
        compiler_params=pltpu.CompilerParams(
            collective_id=0, has_side_effects=True, vmem_limit_bytes=56 * 1024 * 1024
        ),
    )(
        residual.T, mixer_gain.reshape(1, F), lower_bound.reshape(1, 128), head_gain.reshape(1, 128),
        ffn_gain.reshape(1, F), w_query, w_forget, w_input, w_outgate, state.reshape(LOC, 128, 128),
        w_mix_out, w_gate.T, w_up.T, w_down,
    )
    return out.T, new_state.reshape(LOC, 1, 128, 128)


def solution(mesh):
    in_specs = (
        P(None, ("kv", "tp")), P("kv"), P("kv", "tp"), P("kv", "tp"), P("kv", "tp"), P("kv", "tp"), P("tp"),
        P("kv", "tp", None, None), P(), P("tp", "kv"), P("kv"), P("kv", "tp"), P("kv", "tp"), P("tp", "kv"),
    )
    out_specs = (P(None, ("kv", "tp")), P("kv", "tp", None, None))
    return jax.shard_map(body, mesh=mesh, in_specs=in_specs, out_specs=out_specs, check_vma=False)
```

time: 267 us -> 107 us (0.40); the launches traced: 263 us -> 106 us
  Pallas kernels: 0 us -> 101 us
  blocking collectives: 87 us -> 0 us
  waiting for transfers between devices: 69.6 us -> 0 us
  starting transfers between devices: 55.2 us -> 0 us
  other arithmetic: 20.5 us -> 0 us
  local copies, waits for them, and re-layouts: 22.1 us -> 4.43 us
  matrix products: 7.1 us -> 0 us
    pallas_call x0 -> x1, Pallas kernels: none -> 101 us  [body(): pl.pallas_call(layer_kernel, out_shape=(jax.ShapeDtypeStruct((8, SEQ), bf...]
    all_to_all x3 -> x0, blocking collectives: 87 us -> none  [the longest x2 48.3 us: copy_for_each(): return lax.all_to_all(copies, axis, split_axis=0, concat_axis=0, tiled=True)]
    all_to_all x9 -> x0, waiting for transfers between devices: 69.6 us -> none  [the longest x5 38.5 us: summed_on_arrival(): lax.all_to_all(tiles, axis, split_axis=0, concat_axis=0, tiled=True)]
    all_to_all x9 -> x0, starting transfers between devices: 55.2 us -> none  [the longest x5 34.7 us: summed_on_arrival(): lax.all_to_all(tiles, axis, split_axis=0, concat_axis=0, tiled=True)]
    convert_element_type x8 -> x0, local copies, waits for them, and re-layouts: 9.01 us -> none  [the longest x2 6.27 us: body(): rows_float = rows.astype(jnp.float32)]
    dot_general x9 -> x0, matrix products: 7.1 us -> none  [the longest x1 1.87 us: body(): jnp.einsum('shc,shce->she', query, updated, precision=lax.Precision.HIGHEST)]
    broadcast_in_dim x2 -> x0, other arithmetic: 5.5 us -> none  [copy_for_each(): copies = jnp.broadcast_to(shard, (lax.axis_size(axis), *shard.shape))]
    all_to_all x2 -> x0, other arithmetic: 5.5 us -> none  [summed_on_arrival(): lax.all_to_all(tiles, axis, split_axis=0, concat_axis=0, tiled=True)]
  transfers between devices with their start and end apart: 9 -> 0, of which waited for: 8 -> 0; matrix products, arithmetic and copies ran while one was open for 11% -> 0% of each run, Pallas kernels for 0% -> 0%
where the time goes in v1:
time: 107 us; the launch traced here: 106 us
  Pallas kernels  101 us (94%)
  local copies, waits for them, and re-layouts  4.43 us (4%)
    pallas_call x1, Pallas kernels, body(): pl.pallas_call(layer_kernel, out_shape=(jax.ShapeDtypeStruct((8, SEQ), bf...  101 us
    unnamed x2, local copies, waits for them, and re-layouts  4.43 us

profile of v1, /device:TPU:25, one launch (start us, length us, event | category | flops | bytes accessed | tf_op | source)
XLA Modules:
  0.0 105.7 jit_solution(14311054690219794573)
XLA Ops:
  0.6 100.6 %shard_map.149 = (bf16[8,512]{1,0:T(8,128)(2,1)}, f32[32,128,128]{2,1,0:T(8,128)}) custom-call(bf16[8,512]{1,0:T(8,128)(2,1)} %bitcast.16, f32[1,256]{1,0:T(1,128)} %bitcast.18, f32[1,128]{1,0:T(1,128)} %bitcast.20, f32[1,128]{1,0:T(1,128)} %bitcast.21, f32[1,256]{1,0:T(1,128)} %bitcast.19, bf16[256,128]{1,0:T(8,128)(2,1)} %wq_hbm.1, ...), custom_call_target="tpu_custom_call" | custom-call | tf_op jit(solution)/shard_map/pallas_call | solution.py:357
  101.3 1.3 %copy.19 = bf16[512,8]{0,1:T(8,128)(2,1)} copy(bf16[512,8]{0,1:T(8,128)(2,1)} %bitcast.17) | data formatting | bytes 16384
  102.6 3.1 %copy.20 = f32[32,1,128,128]{3,2,1,0:T(8,128)} copy(f32[32,1,128,128]{3,2,1,0:T(8,128)} %bitcast.13) | data formatting | bytes 4194304

commit v2 on v1

v2 whole, which is shorter than its diff:
```python
import jax
import jax.numpy as jnp
from jax import lax
from jax.experimental import pallas as pl
from jax.experimental.pallas import tpu as pltpu
from jax.sharding import PartitionSpec as P

D = 4096
EPS = 1e-06
N = 4
Z = 16
ROWS = 128
LOC = 32
F = 256
FFL = 336
FFP = 384
MESH = pl.DeviceIdType.MESH
NT = (((1,), (1,)), ((), ()))
f32 = jnp.float32
bf16 = jnp.bfloat16


def sigmoid(u):
    return 1.0 / (1.0 + jnp.exp(-u))


def silu(u):
    return u * sigmoid(u)


def z_step(j):
    sign = 1 - 2 * lax.rem(j, 2)
    return 8 + sign * ((j + 1) // 2)


def layer_kernel(
    x_hbm, mg_hbm, lb_hbm, hg_hbm, fg_hbm,
    wq_hbm, wf_hbm, wi_hbm, wo_hbm, state_hbm, wm_hbm, wg_hbm, wu_hbm, wd_hbm,
    out_ref, ns,
    x_ref, mg_ref, lb_ref, hg_ref, fg_ref, wp, wm, wg, wu, wd, gains, st,
    xa, x1, xf, s2, sq2, r2, rq2, qfk, vals, ho, n3, t4, p4, d4, s4, r4, own5, x5, xt5,
    s6, r6, h7, t8, p8, d8, s8, r8, o9,
    wsem, stsem, wps, wpr, wms, wmr, wgs, wgr, wus, wur, wds, wdr, gs, gr, s0s, r0s,
    s1s, r1s, f1s, f1r, s2s, r2s, q2s, q2r, s3s, r3s, d4s, d4r, s4s, r4s,
    s5s, r5s, f5s, f5r, s6s, r6s, s7s, r7s, d8s, d8r, s8s, r8s, s9s, r9s,
):
    k = lax.axis_index("kv")
    t = lax.axis_index("tp")
    z = t // 2
    c = lax.rem(t, 2)
    o = 1 - c
    y = k // N
    x = lax.rem(k, N)
    mate = 2 * z + o

    def turn(a, r):
        return lax.rem(a + r, N)

    def y_to(r):
        return turn(y, r) * N + x

    def x_to(r):
        return y * N + turn(x, r)

    def z_to(r):
        return lax.rem(z + r, Z)

    def z_from(r):
        return lax.rem(z - r + Z, Z)

    def rcopy(src, dst, ssem, rsem, kk, tt):
        return pltpu.make_async_remote_copy(
            src_ref=src, dst_ref=dst, send_sem=ssem, recv_sem=rsem,
            device_id=(kk, tt), device_id_type=MESH,
        )

    def all_sent(view, ssem, rsem):
        rcopy(view, view, ssem, rsem, k, mate).wait_send()

    def all_here(view, ssem, rsem):
        rcopy(view, view, ssem, rsem, k, mate).wait_recv()

    def three(ref):
        return ref.at[pl.ds(0, N - 1)]

    def greet(kk, tt):
        barrier = pltpu.get_barrier_semaphore()
        pl.semaphore_signal(barrier, inc=1, device_id=(kk, tt), device_id_type=MESH)

    def greet_z(j, _):
        greet(k, 2 * z_to(z_step(j)) + c)
        return 0

    lax.fori_loop(0, Z - 1, greet_z, 0)
    for r in range(1, N):
        greet(y_to(r), t)
        greet(x_to(r), t)
    greet(k, mate)

    loads = [
        pltpu.make_async_copy(src, dst, wsem.at[i])
        for i, (src, dst) in enumerate(
            (
                (wq_hbm, wp.at[y, 0]), (wf_hbm, wp.at[y, 1]), (wi_hbm, wp.at[y, 2]), (wo_hbm, wp.at[y, 3]),
                (wm_hbm, wm.at[y]), (wg_hbm, wg.at[y]), (wu_hbm, wu.at[y]), (wd_hbm, wd.at[y]),
                (x_hbm, x_ref), (mg_hbm, mg_ref), (lb_hbm, lb_ref), (hg_hbm, hg_ref), (fg_hbm, fg_ref),
            )
        )
    ]
    for load in loads:
        load.start()
    state_in = pltpu.make_async_copy(state_hbm, st, stsem)
    state_in.start()
    for load in loads:
        load.wait()
    gains[y, 0:1, :] = mg_ref[...]
    gains[y, 1:2, :] = fg_ref[...]
    pl.semaphore_wait(pltpu.get_barrier_semaphore(), (Z - 1) + 2 * (N - 1) + 1)

    for r in range(1, N):
        there = turn(y, r)
        lanes = pl.ds(pl.multiple_of(there * ROWS, ROWS), ROWS)
        rcopy(x_ref.at[:, lanes], xa.at[y], s0s, r0s, y_to(r), t).start()
        rcopy(gains.at[y], gains.at[y], gs, gr, y_to(r), t).start()
    for ref, ss, rs in ((wp, wps, wpr), (wm, wms, wmr), (wg, wgs, wgr), (wu, wus, wur), (wd, wds, wdr)):
        for r in range(1, N):
            rcopy(ref.at[y], ref.at[y], ss, rs, y_to(r), t).start()
    mine = pl.ds(pl.multiple_of(y * ROWS, ROWS), ROWS)
    xa[y] = x_ref[:, mine]
    all_here(three(xa), s0s, r0s)

    def gather_tp(own, slots, ss, rs, fs, fr):
        def send(j, _):
            r = z_step(j)
            rcopy(own, slots.at[t], ss, rs.at[r], k, 2 * z_to(r) + c).start()
            return 0

        lax.fori_loop(0, Z - 1, send, 0)
        rcopy(own, slots.at[t], fs, fr, k, mate).start()

        def forward(i, _):
            r = z_step(Z - 2 - i)
            src = 2 * z_from(r) + c
            rcopy(own, slots.at[src], ss, rs.at[r], k, mate).wait_recv()
            rcopy(slots.at[src], slots.at[src], fs, fr, k, mate).start()
            return 0

        lax.fori_loop(0, Z - 1, forward, 0)
        all_here(slots.at[pl.ds(0, Z)], fs, fr)

    x1[t] = xa[...]
    gather_tp(xa, x1, s1s, r1s, f1s, f1r)
    all_here(three(gains), gs, gr)
    all_here(three(wp), wps, wpr)

    row = jnp.zeros((1, ROWS), f32)
    scaled = []
    for b in range(N):
        xt = x1[:, b].astype(f32).reshape(F, ROWS)
        row = row + jnp.sum(xt * xt, axis=0, keepdims=True)
        rows = xt.T
        xf[b] = rows
        scaled.append((rows * gains[b, 0:1, :]).astype(bf16))
    sq2[...] = jnp.broadcast_to(row, (8, ROWS))
    for i in range(4):
        part = jnp.dot(scaled[0], wp[0, i], preferred_element_type=f32)
        for b in range(1, N):
            part = part + jnp.dot(scaled[b], wp[b, i], preferred_element_type=f32)
        s2[:, :, 128 * i : 128 * i + 128] = part.astype(bf16).reshape(N, LOC, 128)

    for r in range(1, N):
        rcopy(s2.at[turn(x, r)], r2.at[r - 1], s2s, r2s, x_to(r), t).start()
        rcopy(sq2, rq2.at[r - 1], q2s, q2r, x_to(r), t).start()
    state_in.wait()
    all_here(rq2, q2s, q2r)
    all_here(r2, s2s, r2s)

    sq = sq2[...]
    raw = s2[x].astype(f32)
    for i in range(N - 1):
        sq = sq + rq2[i]
        raw = raw + r2[i].astype(f32)
    lane = lax.broadcasted_iota(jnp.int32, (LOC, ROWS), 1)
    seq = lax.broadcasted_iota(jnp.int32, (LOC, ROWS), 0)
    total = jnp.sum(jnp.where(lane == seq + x * LOC, sq[0:1, :], 0.0), axis=1, keepdims=True)
    raw = raw * lax.rsqrt(total / D + EPS)

    bound = lb_ref[...]
    forget_raw = raw[:, 128:256]
    forget = bound + (1.0 - bound) * sigmoid(forget_raw)
    keyvec = (1.0 - bound) * sigmoid(-forget_raw)
    query = silu(raw[:, 0:128])
    vals[...] = raw[:, 256:384]
    out_gate = silu(raw[:, 384:512])
    qfk[...] = jnp.concatenate([query, forget, keyvec, jnp.zeros((LOC, 128), f32)], axis=0).T

    for s in range(LOC):
        new = qfk[:, LOC + s : LOC + s + 1] * st[s] + qfk[:, 2 * LOC + s : 2 * LOC + s + 1] * vals[s : s + 1, :]
        ns[s] = new
        ho[s : s + 1, :] = jnp.sum(qfk[:, s : s + 1] * new, axis=0, keepdims=True)

    head = ho[...]
    inv = lax.rsqrt(jnp.mean(head * head, axis=1, keepdims=True) + EPS)
    n3[x] = (head * inv * hg_ref[...] * out_gate).astype(bf16)

    for r in range(1, N):
        rcopy(n3.at[x], n3.at[x], s3s, r3s, x_to(r), t).start()
    all_here(three(wm), wms, wmr)
    all_here(three(n3), s3s, r3s)

    heads = n3[...].reshape(ROWS, 128)
    for b in range(N):
        mixed = jnp.dot(heads, wm[b], preferred_element_type=f32)
        for i in range(8):
            tt = 8 * b + i
            t4[tt % 2, tt // 2] = mixed[16 * i : 16 * i + 16, :]

    def sum_tp(terms, pairs, got, ring, land, ds_, dr_, ss, rs):
        pairs[...] = terms[o].astype(bf16)
        swap = rcopy(pairs, got, ds_, dr_, k, mate)
        swap.start()
        swap.wait_recv()
        both = terms[c] + got[...].astype(f32)
        ring[...] = both.astype(bf16)
        terms[c] = both

        def send(j, _):
            r = z_step(j)
            zz = z_to(r)
            rcopy(ring.at[zz], land.at[r - 1], ss, rs, k, 2 * zz + c).start()
            return 0

        lax.fori_loop(0, Z - 1, send, 0)
        all_here(land, ss, rs)
        result = terms[c, z]
        for i in range(Z - 1):
            result = result + land[i].astype(f32)
        return result

    summed = sum_tp(t4, p4, d4, s4, r4, d4s, d4r, s4s, r4s)
    block = xf[t // 8, pl.ds(pl.multiple_of(lax.rem(t, 8) * 16, 16), 16), :]
    own5[...] = (block + summed).astype(bf16)
    x5[t] = own5[...]
    gather_tp(own5, x5, s5s, r5s, f5s, f5r)
    all_here(three(wg), wgs, wgr)
    all_here(three(wu), wus, wur)

    squares = jnp.zeros((ROWS, 1), f32)
    scaled = []
    for b in range(N):
        after = x5[8 * b : 8 * b + 8].reshape(ROWS, F).astype(f32)
        squares = squares + jnp.sum(after * after, axis=1, keepdims=True)
        scaled.append((after * gains[b, 1:2, :]).astype(bf16))

    def projected(w):
        acc = lax.dot_general(scaled[0], w[0], NT, preferred_element_type=f32)
        for b in range(1, N):
            acc = acc + lax.dot_general(scaled[b], w[b], NT, preferred_element_type=f32)
        return acc.astype(bf16).reshape(N, LOC, FFL)

    s6[:, :, 0:FFL] = projected(wg)
    s6[:, :, FFP : FFP + FFL] = projected(wu)
    high = squares.astype(bf16).astype(f32)
    spot = lax.broadcasted_iota(jnp.int32, (ROWS, FFP - FFL), 1)
    tail = jnp.where(spot == 0, high, jnp.where(spot == 1, squares - high, 0.0))
    s6[:, :, FFL:FFP] = tail.astype(bf16).reshape(N, LOC, FFP - FFL)
    s6[:, :, FFP + FFL : 2 * FFP] = jnp.zeros((N, LOC, FFP - FFL), bf16)

    for r in range(1, N):
        rcopy(s6.at[turn(x, r)], r6.at[r - 1], s6s, r6s, x_to(r), t).start()
    for b in range(N):
        xt5[b] = x5[8 * b : 8 * b + 8].reshape(ROWS, F).astype(f32).T.reshape(2 * Z, 8, ROWS)
    all_here(r6, s6s, r6s)
    both = s6[x].astype(f32)
    for i in range(N - 1):
        both = both + r6[i].astype(f32)
    total = both[:, FFL : FFL + 1] + both[:, FFL + 1 : FFL + 2]
    inverse = lax.rsqrt(total / D + EPS)
    hidden = silu(both[:, 0:FFP] * inverse) * (both[:, FFP : 2 * FFP] * inverse)
    spot = lax.broadcasted_iota(jnp.int32, (LOC, FFP), 1)
    h7[x] = jnp.where(spot < FFL, hidden, 0.0).astype(bf16)

    for r in range(1, N):
        rcopy(h7.at[x], h7.at[x], s7s, r7s, x_to(r), t).start()
    all_here(three(wd), wds, wdr)
    all_here(three(h7), s7s, r7s)
    hall = h7[...].reshape(ROWS, FFP)[:, 0:FFL]
    for b in range(N):
        down = jnp.dot(hall, wd[b], preferred_element_type=f32).T
        for i in range(2 * Z):
            t8[i % 2, i // 2, b] = down[8 * i : 8 * i + 8, :]

    summed = sum_tp(t8, p8, d8, s8, r8, d8s, d8r, s8s, r8s)
    o9[...] = (xt5[:, t] + summed).astype(bf16)
    for r in range(1, N):
        rcopy(o9.at[turn(y, r)], out_ref.at[:, mine], s9s, r9s, y_to(r), t).start()
    out_ref[:, mine] = o9[y]
    three_out = out_ref.at[:, pl.ds(0, (N - 1) * ROWS)]
    all_here(three_out, s9s, r9s)

    all_sent(three(xa), s0s, r0s)
    all_sent(three(gains), gs, gr)
    for ref, ss, rs in ((wp, wps, wpr), (wm, wms, wmr), (wg, wgs, wgr), (wu, wus, wur), (wd, wds, wdr)):
        all_sent(three(ref), ss, rs)
    all_sent(x1.at[pl.ds(0, Z - 1)], s1s, r1s.at[0])
    all_sent(x1.at[pl.ds(0, Z)], f1s, f1r)
    all_sent(r2, s2s, r2s)
    all_sent(rq2, q2s, q2r)
    all_sent(three(n3), s3s, r3s)
    all_sent(p4, d4s, d4r)
    all_sent(r4, s4s, r4s)
    all_sent(x5.at[pl.ds(0, Z - 1)], s5s, r5s.at[0])
    all_sent(x5.at[pl.ds(0, Z)], f5s, f5r)
    all_sent(r6, s6s, r6s)
    all_sent(three(h7), s7s, r7s)
    all_sent(p8, d8s, d8r)
    all_sent(r8, s8s, r8s)
    all_sent(three_out, s9s, r9s)


def body(
    residual, mixer_gain, w_query, w_forget, w_input, w_outgate, lower_bound, state, head_gain,
    w_mix_out, ffn_gain, w_gate, w_up, w_down,
):
    vmem = pl.BlockSpec(memory_space=pltpu.VMEM)
    hbm = pl.BlockSpec(memory_space=pltpu.HBM)
    V = pltpu.VMEM
    dma = pltpu.SemaphoreType.DMA
    ring = [V((Z, 16, F), bf16), V((Z, 16, F), bf16), V((Z, 16, F), bf16), V((Z - 1, 16, F), bf16)]
    ring8 = [V((Z, N, 8, ROWS), bf16)] * 3 + [V((Z - 1, N, 8, ROWS), bf16)]
    scratch = [
        V((8, 4 * ROWS), bf16), V((1, F), f32), V((1, 128), f32), V((1, 128), f32), V((1, F), f32),
        V((N, 4, F, 128), bf16), V((N, 128, F), bf16), V((N, FFL, F), bf16), V((N, FFL, F), bf16), V((N, FFL, F), bf16),
        V((N, 2, F), f32), V((LOC, 128, 128), f32),
        V((N, 8, ROWS), bf16), V((2 * Z, N, 8, ROWS), bf16), V((N, ROWS, F), f32),
        V((N, LOC, 512), bf16), V((8, ROWS), f32), V((N - 1, LOC, 512), bf16), V((N - 1, 8, ROWS), f32),
        V((128, 128), f32), V((LOC, 128), f32), V((LOC, 128), f32),
        V((N, LOC, 128), bf16),
        V((2, Z, 16, F), f32), *ring,
        V((16, F), bf16), V((2 * Z, 16, F), bf16), V((N, 2 * Z, 8, ROWS), f32),
        V((N, LOC, 2 * FFP), bf16), V((N - 1, LOC, 2 * FFP), bf16), V((N, LOC, FFP), bf16),
        V((2, Z, N, 8, ROWS), f32), *ring8, V((N, 8, ROWS), bf16),
        dma((13,)), dma, *([dma] * 14),
        dma, dma((Z,)), *([dma] * 12),
        dma, dma((Z,)), *([dma] * 12),
    ]
    out, new_state = pl.pallas_call(
        layer_kernel,
        out_shape=(
            jax.ShapeDtypeStruct((8, 4 * ROWS), bf16),
            jax.ShapeDtypeStruct((LOC, 128, 128), f32),
        ),
        in_specs=[hbm] * 14,
        out_specs=(vmem, vmem),
        scratch_shapes=scratch,
        compiler_params=pltpu.CompilerParams(
            collective_id=0, has_side_effects=True, vmem_limit_bytes=24 * 1024 * 1024
        ),
    )(
        *(
            pltpu.with_memory_space_constraint(a, pltpu.HBM)
            for a in (
                residual.T, mixer_gain.reshape(1, F), lower_bound.reshape(1, 128), head_gain.reshape(1, 128),
                ffn_gain.reshape(1, F), w_query, w_forget, w_input, w_outgate, state.reshape(LOC, 128, 128),
                w_mix_out, w_gate.T, w_up.T, w_down,
            )
        ),
    )
    return out.T, new_state.reshape(LOC, 1, 128, 128)


def solution(mesh):
    in_specs = (
        P(None, ("kv", "tp")), P("kv"), P("kv", "tp"), P("kv", "tp"), P("kv", "tp"), P("kv", "tp"), P("tp"),
        P("kv", "tp", None, None), P(), P("tp", "kv"), P("kv"), P("kv", "tp"), P("kv", "tp"), P("tp", "kv"),
    )
    out_specs = (P(None, ("kv", "tp")), P("kv", "tp", None, None))
    return jax.shard_map(body, mesh=mesh, in_specs=in_specs, out_specs=out_specs, check_vma=False)
```

time: 107 us -> 87.3 us (0.82)
  Pallas kernels: 101 us -> 83.4 us
  local copies, waits for them, and re-layouts: 4.43 us -> 1.92 us
    pallas_call x1, Pallas kernels: 101 us -> 83.4 us  [body(): pl.pallas_call(layer_kernel, out_shape=(jax.ShapeDtypeStruct((8, 4 * ROWS...]
    unnamed x2, local copies, waits for them, and re-layouts: 4.43 us -> 1.92 us
where the time goes in v2:
time: 87.3 us; the launch traced here: 86 us
  Pallas kernels  83.4 us (96%)
  local copies, waits for them, and re-layouts  1.92 us (2%)
    pallas_call x1, Pallas kernels, body(): pl.pallas_call(layer_kernel, out_shape=(jax.ShapeDtypeStruct((8, 4 * ROWS...  83.4 us
    unnamed x2, local copies, waits for them, and re-layouts  1.92 us

profile of v2, /device:TPU:25, one launch (start us, length us, event | category | flops | bytes accessed | tf_op | source)
XLA Modules:
  0.0 86.0 jit_solution(1649494835232264769)
XLA Ops:
  0.6 83.4 %shard_map.149 = (bf16[8,512]{1,0:T(8,128)(2,1)S(1)}, f32[32,128,128]{2,1,0:T(8,128)S(1)}) custom-call(bf16[8,512]{1,0:T(8,128)(2,1)} %bitcast.17, f32[1,256]{1,0:T(1,128)} %bitcast.18, f32[1,128]{1,0:T(1,128)} %bitcast.20, f32[1,128]{1,0:T(1,128)} %bitcast.21, f32[1,256]{1,0:T(1,128)} %bitcast.19, bf16[256,128]{1,0:T(8,128)(2,1)} %wq_hbm.1, ...), custom_call_target="tpu_custom_call" | custom-call | tf_op jit(solution)/shard_map/pallas_call | solution.py:347
  84.0 0.6 copy.19
  84.6 1.3 %copy.20 = f32[32,1,128,128]{3,2,1,0:T(8,128)} copy(f32[32,1,128,128]{3,2,1,0:T(8,128)S(1)} %bitcast.12) | data formatting | bytes 4194304

commit v3 on v2

--- a/solution.py
+++ b/solution.py
@@ -38,11 +38,11 @@
     wq_hbm, wf_hbm, wi_hbm, wo_hbm, state_hbm, wm_hbm, wg_hbm, wu_hbm, wd_hbm,
     out_ref, ns,
     x_ref, mg_ref, lb_ref, hg_ref, fg_ref, wp, wm, wg, wu, wd, gains, st,
-    xa, x1, xf, s2, sq2, r2, rq2, qfk, vals, ho, n3, t4, p4, d4, s4, r4, own5, x5, xt5,
-    s6, r6, h7, t8, p8, d8, s8, r8, o9,
+    xa, x1, xf, s2, sq2, r2, rq2, qfk, vals, ho, n3, t4, s4, r4, own5, x5, xt5,
+    s6, r6, h7, t8, p8, d8, s8, r8,
     wsem, stsem, wps, wpr, wms, wmr, wgs, wgr, wus, wur, wds, wdr, gs, gr, s0s, r0s,
-    s1s, r1s, f1s, f1r, s2s, r2s, q2s, q2r, s3s, r3s, d4s, d4r, s4s, r4s,
-    s5s, r5s, f5s, f5r, s6s, r6s, s7s, r7s, d8s, d8r, s8s, r8s, s9s, r9s,
+    s1s, r1s, f1s, f1r, s2s, r2s, q2s, q2r, s3s, r3s, ms, mr, s4s, r4s,
+    s5s, r5s, f5s, f5r, s6s, r6s, s7s, r7s, d8s, d8r, s8s, r8s,
 ):
     k = lax.axis_index("kv")
     t = lax.axis_index("tp")
@@ -102,7 +102,7 @@
         for i, (src, dst) in enumerate(
             (
                 (wq_hbm, wp.at[y, 0]), (wf_hbm, wp.at[y, 1]), (wi_hbm, wp.at[y, 2]), (wo_hbm, wp.at[y, 3]),
-                (wm_hbm, wm.at[y]), (wg_hbm, wg.at[y]), (wu_hbm, wu.at[y]), (wd_hbm, wd.at[y]),
+                (wm_hbm, wm.at[c, y]), (wg_hbm, wg.at[y]), (wu_hbm, wu.at[y]), (wd_hbm, wd.at[y]),
                 (x_hbm, x_ref), (mg_hbm, mg_ref), (lb_hbm, lb_ref), (hg_hbm, hg_ref), (fg_hbm, fg_ref),
             )
         )
@@ -122,25 +122,25 @@
         lanes = pl.ds(pl.multiple_of(there * ROWS, ROWS), ROWS)
         rcopy(x_ref.at[:, lanes], xa.at[y], s0s, r0s, y_to(r), t).start()
         rcopy(gains.at[y], gains.at[y], gs, gr, y_to(r), t).start()
-    for ref, ss, rs in ((wp, wps, wpr), (wm, wms, wmr), (wg, wgs, wgr), (wu, wus, wur), (wd, wds, wdr)):
+    for ref, ss, rs in ((wp, wps, wpr), (wm.at[c], wms, wmr), (wg, wgs, wgr), (wu, wus, wur), (wd, wds, wdr)):
         for r in range(1, N):
             rcopy(ref.at[y], ref.at[y], ss, rs, y_to(r), t).start()
     mine = pl.ds(pl.multiple_of(y * ROWS, ROWS), ROWS)
     xa[y] = x_ref[:, mine]
     all_here(three(xa), s0s, r0s)
 
-    def gather_tp(own, slots, ss, rs, fs, fr):
+    def gather_tp(own, slots, slot, ss, rs, fs, fr):
         def send(j, _):
             r = z_step(j)
-            rcopy(own, slots.at[t], ss, rs.at[r], k, 2 * z_to(r) + c).start()
+            rcopy(own, slots.at[slot(z, c)], ss, rs.at[r], k, 2 * z_to(r) + c).start()
             return 0
 
         lax.fori_loop(0, Z - 1, send, 0)
-        rcopy(own, slots.at[t], fs, fr, k, mate).start()
+        rcopy(own, slots.at[slot(z, c)], fs, fr, k, mate).start()
 
         def forward(i, _):
             r = z_step(Z - 2 - i)
-            src = 2 * z_from(r) + c
+            src = slot(z_from(r), c)
             rcopy(own, slots.at[src], ss, rs.at[r], k, mate).wait_recv()
             rcopy(slots.at[src], slots.at[src], fs, fr, k, mate).start()
             return 0
@@ -149,7 +149,7 @@
         all_here(slots.at[pl.ds(0, Z)], fs, fr)
 
     x1[t] = xa[...]
-    gather_tp(xa, x1, s1s, r1s, f1s, f1r)
+    gather_tp(xa, x1, lambda zz, cc: 2 * zz + cc, s1s, r1s, f1s, f1r)
     all_here(three(gains), gs, gr)
     all_here(three(wp), wps, wpr)
 
@@ -171,6 +171,8 @@
     for r in range(1, N):
         rcopy(s2.at[turn(x, r)], r2.at[r - 1], s2s, r2s, x_to(r), t).start()
         rcopy(sq2, rq2.at[r - 1], q2s, q2r, x_to(r), t).start()
+    all_here(three(wm.at[c]), wms, wmr)
+    rcopy(wm.at[c], wm.at[c], ms, mr, k, mate).start()
     state_in.wait()
     all_here(rq2, q2s, q2r)
     all_here(r2, s2s, r2s)
@@ -192,56 +194,54 @@
     query = silu(raw[:, 0:128])
     vals[...] = raw[:, 256:384]
     out_gate = silu(raw[:, 384:512])
-    qfk[...] = jnp.concatenate([query, forget, keyvec, jnp.zeros((LOC, 128), f32)], axis=0).T
+    qfk[...] = jnp.concatenate([query * forget, forget, keyvec, jnp.zeros((LOC, 128), f32)], axis=0).T
+    weight = jnp.sum(query * keyvec, axis=1, keepdims=True)
 
     for s in range(LOC):
-        new = qfk[:, LOC + s : LOC + s + 1] * st[s] + qfk[:, 2 * LOC + s : 2 * LOC + s + 1] * vals[s : s + 1, :]
-        ns[s] = new
-        ho[s : s + 1, :] = jnp.sum(qfk[:, s : s + 1] * new, axis=0, keepdims=True)
-
-    head = ho[...]
+        ho[s : s + 1, :] = jnp.sum(qfk[:, s : s + 1] * st[s], axis=0, keepdims=True)
+
+    head = ho[...] + weight * vals[...]
     inv = lax.rsqrt(jnp.mean(head * head, axis=1, keepdims=True) + EPS)
-    n3[x] = (head * inv * hg_ref[...] * out_gate).astype(bf16)
-
-    for r in range(1, N):
-        rcopy(n3.at[x], n3.at[x], s3s, r3s, x_to(r), t).start()
-    all_here(three(wm), wms, wmr)
-    all_here(three(n3), s3s, r3s)
-
-    heads = n3[...].reshape(ROWS, 128)
-    for b in range(N):
-        mixed = jnp.dot(heads, wm[b], preferred_element_type=f32)
-        for i in range(8):
-            tt = 8 * b + i
-            t4[tt % 2, tt // 2] = mixed[16 * i : 16 * i + 16, :]
-
-    def sum_tp(terms, pairs, got, ring, land, ds_, dr_, ss, rs):
-        pairs[...] = terms[o].astype(bf16)
-        swap = rcopy(pairs, got, ds_, dr_, k, mate)
-        swap.start()
-        swap.wait_recv()
-        both = terms[c] + got[...].astype(f32)
-        ring[...] = both.astype(bf16)
-        terms[c] = both
-
-        def send(j, _):
-            r = z_step(j)
-            zz = z_to(r)
-            rcopy(ring.at[zz], land.at[r - 1], ss, rs, k, 2 * zz + c).start()
-            return 0
-
-        lax.fori_loop(0, Z - 1, send, 0)
-        all_here(land, ss, rs)
-        result = terms[c, z]
-        for i in range(Z - 1):
-            result = result + land[i].astype(f32)
-        return result
-
-    summed = sum_tp(t4, p4, d4, s4, r4, d4s, d4r, s4s, r4s)
-    block = xf[t // 8, pl.ds(pl.multiple_of(lax.rem(t, 8) * 16, 16), 16), :]
-    own5[...] = (block + summed).astype(bf16)
-    x5[t] = own5[...]
-    gather_tp(own5, x5, s5s, r5s, f5s, f5r)
+    n3[2 * x + c] = (head * inv * hg_ref[...] * out_gate).astype(bf16)
+
+    mine3 = n3.at[2 * x + c]
+    for r in range(1, N):
+        rcopy(mine3, mine3, s3s, r3s, x_to(r), t).start()
+        rcopy(mine3, mine3, s3s, r3s, x_to(r), mate).start()
+    rcopy(mine3, mine3, s3s, r3s, k, mate).start()
+    for s in range(LOC):
+        ns[s] = (
+            qfk[:, LOC + s : LOC + s + 1] * st[s]
+            + qfk[:, 2 * LOC + s : 2 * LOC + s + 1] * vals[s : s + 1, :]
+        )
+    all_here(wm.at[o], ms, mr)
+    all_here(n3.at[pl.ds(0, 2 * N - 1)], s3s, r3s)
+
+    heads = [jnp.concatenate([n3[4 * c + i], n3[4 * c + 2 + i]], axis=0) for i in range(2)]
+    for b in range(N):
+        mixed = jnp.dot(heads[0], wm[0, b], preferred_element_type=f32)
+        mixed = mixed + jnp.dot(heads[1], wm[1, b], preferred_element_type=f32)
+        for i in range(4):
+            t4[4 * b + i] = mixed[16 * i : 16 * i + 16, :]
+            s4[4 * b + i] = mixed[16 * i : 16 * i + 16, :].astype(bf16)
+
+    def block_of(zz, cc):
+        return (zz // 4) * 8 + cc * 4 + lax.rem(zz, 4)
+
+    def send4(j, _):
+        r = z_step(j)
+        zz = z_to(r)
+        rcopy(s4.at[zz], r4.at[r - 1], s4s, r4s, k, 2 * zz + c).start()
+        return 0
+
+    lax.fori_loop(0, Z - 1, send4, 0)
+    block = xf[z // 4, pl.ds(pl.multiple_of(c * 64 + lax.rem(z, 4) * 16, 16), 16), :] + t4[z]
+    all_here(r4, s4s, r4s)
+    for i in range(Z - 1):
+        block = block + r4[i].astype(f32)
+    own5[...] = block.astype(bf16)
+    x5[block_of(z, c)] = own5[...]
+    gather_tp(own5, x5, block_of, s5s, r5s, f5s, f5r)
     all_here(three(wg), wgs, wgr)
     all_here(three(wu), wus, wur)
 
@@ -290,32 +290,65 @@
         for i in range(2 * Z):
             t8[i % 2, i // 2, b] = down[8 * i : 8 * i + 8, :]
 
-    summed = sum_tp(t8, p8, d8, s8, r8, d8s, d8r, s8s, r8s)
-    o9[...] = (xt5[:, t] + summed).astype(bf16)
-    for r in range(1, N):
-        rcopy(o9.at[turn(y, r)], out_ref.at[:, mine], s9s, r9s, y_to(r), t).start()
-    out_ref[:, mine] = o9[y]
-    three_out = out_ref.at[:, pl.ds(0, (N - 1) * ROWS)]
-    all_here(three_out, s9s, r9s)
+    p8[...] = t8[o].astype(bf16)
+    swap = rcopy(p8, d8, d8s, d8r, k, mate)
+    swap.start()
+    t8[c, z] = t8[c, z] + xt5[:, t]
+    swap.wait_recv()
+    s8[...] = (t8[c] + d8[...].astype(f32)).astype(bf16)
+
+    def piece(r, q):
+        zz = z_to(r)
+        there = turn(y, q)
+        rcopy(s8.at[zz, there], r8.at[y * Z + r], s8s, r8s, there * N + x, 2 * zz + c).start()
+
+    def send8(j, _):
+        for q in range(N):
+            piece(z_step(j), q)
+        return 0
+
+    lax.fori_loop(0, Z - 1, send8, 0)
+    for q in range(1, N):
+        piece(0, q)
+    r8[y * Z] = s8[z, y]
+    pieces = r8.at[pl.ds(0, N * Z - 1)]
+    all_here(pieces, s8s, r8s)
+    for b in range(N):
+        acc = r8[b * Z].astype(f32)
+        for i in range(1, Z):
+            acc = acc + r8[b * Z + i].astype(f32)
+        out_ref[:, ROWS * b : ROWS * b + ROWS] = acc.astype(bf16)
 
     all_sent(three(xa), s0s, r0s)
     all_sent(three(gains), gs, gr)
-    for ref, ss, rs in ((wp, wps, wpr), (wm, wms, wmr), (wg, wgs, wgr), (wu, wus, wur), (wd, wds, wdr)):
+    for ref, ss, rs in ((wp, wps, wpr), (wm.at[c], wms, wmr), (wg, wgs, wgr), (wu, wus, wur), (wd, wds, wdr)):
         all_sent(three(ref), ss, rs)
+    all_sent(wm.at[c], ms, mr)
     all_sent(x1.at[pl.ds(0, Z - 1)], s1s, r1s.at[0])
     all_sent(x1.at[pl.ds(0, Z)], f1s, f1r)
     all_sent(r2, s2s, r2s)
     all_sent(rq2, q2s, q2r)
-    all_sent(three(n3), s3s, r3s)
-    all_sent(p4, d4s, d4r)
+    all_sent(n3.at[pl.ds(0, 2 * N - 1)], s3s, r3s)
     all_sent(r4, s4s, r4s)
     all_sent(x5.at[pl.ds(0, Z - 1)], s5s, r5s.at[0])
     all_sent(x5.at[pl.ds(0, Z)], f5s, f5r)
     all_sent(r6, s6s, r6s)
     all_sent(three(h7), s7s, r7s)
     all_sent(p8, d8s, d8r)
-    all_sent(r8, s8s, r8s)
-    all_sent(three_out, s9s, r9s)
+    all_sent(pieces, s8s, r8s)
+
+
+def write_out(out_ref, ns_ref, out_hbm, ns_hbm, sems):
+    part = LOC // 4
+    copies = [
+        pltpu.make_async_copy(ns_ref.at[pl.ds(part * i, part)], ns_hbm.at[pl.ds(part * i, part)], sems.at[i])
+        for i in range(4)
+    ]
+    copies.append(pltpu.make_async_copy(out_ref, out_hbm, sems.at[4]))
+    for copy in copies:
+        copy.start()
+    for copy in copies:
+        copy.wait()
 
 
 def body(
@@ -326,23 +359,22 @@
     hbm = pl.BlockSpec(memory_space=pltpu.HBM)
     V = pltpu.VMEM
     dma = pltpu.SemaphoreType.DMA
-    ring = [V((Z, 16, F), bf16), V((Z, 16, F), bf16), V((Z, 16, F), bf16), V((Z - 1, 16, F), bf16)]
-    ring8 = [V((Z, N, 8, ROWS), bf16)] * 3 + [V((Z - 1, N, 8, ROWS), bf16)]
+    ring8 = [V((Z, N, 8, ROWS), bf16)] * 3 + [V((N * Z, 8, ROWS), bf16)]
     scratch = [
         V((8, 4 * ROWS), bf16), V((1, F), f32), V((1, 128), f32), V((1, 128), f32), V((1, F), f32),
-        V((N, 4, F, 128), bf16), V((N, 128, F), bf16), V((N, FFL, F), bf16), V((N, FFL, F), bf16), V((N, FFL, F), bf16),
+        V((N, 4, F, 128), bf16), V((2, N, 128, F), bf16), V((N, FFL, F), bf16), V((N, FFL, F), bf16), V((N, FFL, F), bf16),
         V((N, 2, F), f32), V((LOC, 128, 128), f32),
         V((N, 8, ROWS), bf16), V((2 * Z, N, 8, ROWS), bf16), V((N, ROWS, F), f32),
         V((N, LOC, 512), bf16), V((8, ROWS), f32), V((N - 1, LOC, 512), bf16), V((N - 1, 8, ROWS), f32),
         V((128, 128), f32), V((LOC, 128), f32), V((LOC, 128), f32),
-        V((N, LOC, 128), bf16),
-        V((2, Z, 16, F), f32), *ring,
+        V((2 * N, LOC, 128), bf16),
+        V((Z, 16, F), f32), V((Z, 16, F), bf16), V((Z - 1, 16, F), bf16),
         V((16, F), bf16), V((2 * Z, 16, F), bf16), V((N, 2 * Z, 8, ROWS), f32),
         V((N, LOC, 2 * FFP), bf16), V((N - 1, LOC, 2 * FFP), bf16), V((N, LOC, FFP), bf16),
-        V((2, Z, N, 8, ROWS), f32), *ring8, V((N, 8, ROWS), bf16),
+        V((2, Z, N, 8, ROWS), f32), *ring8,
         dma((13,)), dma, *([dma] * 14),
         dma, dma((Z,)), *([dma] * 12),
-        dma, dma((Z,)), *([dma] * 12),
+        dma, dma((Z,)), *([dma] * 10),
     ]
     out, new_state = pl.pallas_call(
         layer_kernel,
@@ -366,6 +398,17 @@
             )
         ),
     )
+    out, new_state = pl.pallas_call(
+        write_out,
+        out_shape=(
+            jax.ShapeDtypeStruct((8, 4 * ROWS), bf16),
+            jax.ShapeDtypeStruct((LOC, 128, 128), f32),
+        ),
+        in_specs=[vmem] * 2,
+        out_specs=(hbm, hbm),
+        scratch_shapes=[dma((5,))],
+        compiler_params=pltpu.CompilerParams(vmem_limit_bytes=8 * 1024 * 1024),
+    )(out, new_state)
     return out.T, new_state.reshape(LOC, 1, 128, 128)
 
 

time: 87.3 us -> 82.2 us (0.942)
  Pallas kernels: 83.4 us -> 80.5 us
  local copies, waits for them, and re-layouts: 1.92 us -> 0 us
    pallas_call x1, Pallas kernels: 83.4 us -> 79.1 us  [body(): pl.pallas_call(layer_kernel, out_shape=(jax.ShapeDtypeStruct((8, 4 * ROWS...]
    unnamed x2 -> x0, local copies, waits for them, and re-layouts: 1.92 us -> none
    pallas_call x0 -> x1, Pallas kernels: none -> 1.36 us  [body(): pl.pallas_call(write_out, out_shape=(jax.ShapeDtypeStruct((8, 4 * ROWS),...]
where the time goes in v3:
time: 82.2 us; the launch traced here: 81.1 us
  Pallas kernels  80.5 us (98%)
    pallas_call x1, Pallas kernels, body(): pl.pallas_call(layer_kernel, out_shape=(jax.ShapeDtypeStruct((8, 4 * ROWS...  79.1 us

profile of v3, /device:TPU:25, one launch (start us, length us, event | category | flops | bytes accessed | tf_op | source)
XLA Modules:
  0.0 81.1 jit_solution(7931430079585450916)
XLA Ops:
  0.6 79.1 %shard_map.149 = (bf16[8,512]{1,0:T(8,128)(2,1)S(1)}, f32[32,128,128]{2,1,0:T(8,128)S(1)}) custom-call(bf16[8,512]{1,0:T(8,128)(2,1)} %bitcast.15, f32[1,256]{1,0:T(1,128)} %bitcast.16, f32[1,128]{1,0:T(1,128)} %bitcast.18, f32[1,128]{1,0:T(1,128)} %bitcast.19, f32[1,256]{1,0:T(1,128)} %bitcast.17, bf16[256,128]{1,0:T(8,128)(2,1)} %wq_hbm.1, ...), custom_call_target="tpu_custom_call" | custom-call | tf_op jit(solution)/shard_map/pallas_call | solution.py:379
  79.7 1.4 %shard_map.150 = (bf16[8,512]{1,0:T(8,128)(2,1)}, f32[32,128,128]{2,1,0:T(8,128)}) custom-call(bf16[8,512]{1,0:T(8,128)(2,1)S(1)} %get-tuple-element.6.out_ref, f32[32,128,128]{2,1,0:T(8,128)S(1)} %get-tuple-element.7.ns_ref), custom_call_target="tpu_custom_call" | custom-call | tf_op jit(solution)/shard_map/pallas_call | solution.py:401

commit v4 on v3

--- a/solution.py
+++ b/solution.py
@@ -37,10 +37,10 @@
     x_hbm, mg_hbm, lb_hbm, hg_hbm, fg_hbm,
     wq_hbm, wf_hbm, wi_hbm, wo_hbm, state_hbm, wm_hbm, wg_hbm, wu_hbm, wd_hbm,
     out_ref, ns,
-    x_ref, mg_ref, lb_ref, hg_ref, fg_ref, wp, wm, wg, wu, wd, gains, st,
-    xa, x1, xf, s2, sq2, r2, rq2, qfk, vals, ho, n3, t4, s4, r4, own5, x5, xt5,
+    x_ref, mg_ref, lb_ref, hg_ref, fg_ref, wp, wo, wm, wg, wu, wd, gains, st,
+    xa, x1, xf, s2, sq2, r2, rq2, s2b, r2b, qfk, vals, ho, n3, t4, s4, r4, own5, x5, xt5,
     s6, r6, h7, t8, p8, d8, s8, r8,
-    wsem, stsem, wps, wpr, wms, wmr, wgs, wgr, wus, wur, wds, wdr, gs, gr, s0s, r0s,
+    word, wsem, stsem, wps, wpr, wos, wor, wms, wmr, wgs, wgr, wus, wur, wds, wdr, gs, gr, s0s, r0s, b2s, b2r,
     s1s, r1s, f1s, f1r, s2s, r2s, q2s, q2r, s3s, r3s, ms, mr, s4s, r4s,
     s5s, r5s, f5s, f5r, s6s, r6s, s7s, r7s, d8s, d8r, s8s, r8s,
 ):
@@ -87,11 +87,9 @@
         barrier = pltpu.get_barrier_semaphore()
         pl.semaphore_signal(barrier, inc=1, device_id=(kk, tt), device_id_type=MESH)
 
-    def greet_z(j, _):
-        greet(k, 2 * z_to(z_step(j)) + c)
-        return 0
-
-    lax.fori_loop(0, Z - 1, greet_z, 0)
+    for d in range(4, 0, -1):
+        greet(k, 2 * z_to(d) + c)
+        greet(k, 2 * z_to(Z - d) + c)
     for r in range(1, N):
         greet(y_to(r), t)
         greet(x_to(r), t)
@@ -101,7 +99,7 @@
         pltpu.make_async_copy(src, dst, wsem.at[i])
         for i, (src, dst) in enumerate(
             (
-                (wq_hbm, wp.at[y, 0]), (wf_hbm, wp.at[y, 1]), (wi_hbm, wp.at[y, 2]), (wo_hbm, wp.at[y, 3]),
+                (wq_hbm, wp.at[y, 0]), (wf_hbm, wp.at[y, 1]), (wi_hbm, wp.at[y, 2]), (wo_hbm, wo.at[y]),
                 (wm_hbm, wm.at[c, y]), (wg_hbm, wg.at[y]), (wu_hbm, wu.at[y]), (wd_hbm, wd.at[y]),
                 (x_hbm, x_ref), (mg_hbm, mg_ref), (lb_hbm, lb_ref), (hg_hbm, hg_ref), (fg_hbm, fg_ref),
             )
@@ -115,19 +113,23 @@
         load.wait()
     gains[y, 0:1, :] = mg_ref[...]
     gains[y, 1:2, :] = fg_ref[...]
-    pl.semaphore_wait(pltpu.get_barrier_semaphore(), (Z - 1) + 2 * (N - 1) + 1)
+    pl.semaphore_wait(pltpu.get_barrier_semaphore(), 8 + 2 * (N - 1) + 1)
+
+    pl.semaphore_signal(word, inc=1, device_id=(k, 2 * z_to(4) + c), device_id_type=MESH)
+    pl.semaphore_signal(word, inc=1, device_id=(k, 2 * z_to(Z - 4) + c), device_id_type=MESH)
 
     for r in range(1, N):
         there = turn(y, r)
         lanes = pl.ds(pl.multiple_of(there * ROWS, ROWS), ROWS)
         rcopy(x_ref.at[:, lanes], xa.at[y], s0s, r0s, y_to(r), t).start()
         rcopy(gains.at[y], gains.at[y], gs, gr, y_to(r), t).start()
-    for ref, ss, rs in ((wp, wps, wpr), (wm.at[c], wms, wmr), (wg, wgs, wgr), (wu, wus, wur), (wd, wds, wdr)):
+    for ref, ss, rs in ((wp, wps, wpr), (wo, wos, wor), (wm.at[c], wms, wmr), (wg, wgs, wgr), (wu, wus, wur), (wd, wds, wdr)):
         for r in range(1, N):
             rcopy(ref.at[y], ref.at[y], ss, rs, y_to(r), t).start()
     mine = pl.ds(pl.multiple_of(y * ROWS, ROWS), ROWS)
     xa[y] = x_ref[:, mine]
     all_here(three(xa), s0s, r0s)
+    pl.semaphore_wait(word, 2)
 
     def gather_tp(own, slots, slot, ss, rs, fs, fr):
         def send(j, _):
@@ -162,15 +164,23 @@
         xf[b] = rows
         scaled.append((rows * gains[b, 0:1, :]).astype(bf16))
     sq2[...] = jnp.broadcast_to(row, (8, ROWS))
-    for i in range(4):
-        part = jnp.dot(scaled[0], wp[0, i], preferred_element_type=f32)
+
+    def projection(w):
+        part = jnp.dot(scaled[0], w(0), preferred_element_type=f32)
         for b in range(1, N):
-            part = part + jnp.dot(scaled[b], wp[b, i], preferred_element_type=f32)
-        s2[:, :, 128 * i : 128 * i + 128] = part.astype(bf16).reshape(N, LOC, 128)
+            part = part + jnp.dot(scaled[b], w(b), preferred_element_type=f32)
+        return part.astype(bf16).reshape(N, LOC, 128)
+
+    for i in range(3):
+        s2[:, :, 128 * i : 128 * i + 128] = projection(lambda b, i=i: wp[b, i])
 
     for r in range(1, N):
         rcopy(s2.at[turn(x, r)], r2.at[r - 1], s2s, r2s, x_to(r), t).start()
         rcopy(sq2, rq2.at[r - 1], q2s, q2r, x_to(r), t).start()
+    all_here(three(wo), wos, wor)
+    s2b[...] = projection(lambda b: wo[b])
+    for r in range(1, N):
+        rcopy(s2b.at[turn(x, r)], r2b.at[r - 1], b2s, b2r, x_to(r), t).start()
     all_here(three(wm.at[c]), wms, wmr)
     rcopy(wm.at[c], wm.at[c], ms, mr, k, mate).start()
     state_in.wait()
@@ -185,7 +195,8 @@
     lane = lax.broadcasted_iota(jnp.int32, (LOC, ROWS), 1)
     seq = lax.broadcasted_iota(jnp.int32, (LOC, ROWS), 0)
     total = jnp.sum(jnp.where(lane == seq + x * LOC, sq[0:1, :], 0.0), axis=1, keepdims=True)
-    raw = raw * lax.rsqrt(total / D + EPS)
+    inv_a = lax.rsqrt(total / D + EPS)
+    raw = raw * inv_a
 
     bound = lb_ref[...]
     forget_raw = raw[:, 128:256]
@@ -193,13 +204,17 @@
     keyvec = (1.0 - bound) * sigmoid(-forget_raw)
     query = silu(raw[:, 0:128])
     vals[...] = raw[:, 256:384]
-    out_gate = silu(raw[:, 384:512])
     qfk[...] = jnp.concatenate([query * forget, forget, keyvec, jnp.zeros((LOC, 128), f32)], axis=0).T
     weight = jnp.sum(query * keyvec, axis=1, keepdims=True)
 
     for s in range(LOC):
         ho[s : s + 1, :] = jnp.sum(qfk[:, s : s + 1] * st[s], axis=0, keepdims=True)
 
+    all_here(r2b, b2s, b2r)
+    raw = s2b[x].astype(f32)
+    for i in range(N - 1):
+        raw = raw + r2b[i].astype(f32)
+    out_gate = silu(raw * inv_a)
     head = ho[...] + weight * vals[...]
     inv = lax.rsqrt(jnp.mean(head * head, axis=1, keepdims=True) + EPS)
     n3[2 * x + c] = (head * inv * hg_ref[...] * out_gate).astype(bf16)
@@ -258,25 +273,27 @@
             acc = acc + lax.dot_general(scaled[b], w[b], NT, preferred_element_type=f32)
         return acc.astype(bf16).reshape(N, LOC, FFL)
 
-    s6[:, :, 0:FFL] = projected(wg)
-    s6[:, :, FFP : FFP + FFL] = projected(wu)
+    s6[:, 0, :, 0:FFL] = projected(wg)
+    s6[:, 1, :, 0:FFL] = projected(wu)
     high = squares.astype(bf16).astype(f32)
     spot = lax.broadcasted_iota(jnp.int32, (ROWS, FFP - FFL), 1)
     tail = jnp.where(spot == 0, high, jnp.where(spot == 1, squares - high, 0.0))
-    s6[:, :, FFL:FFP] = tail.astype(bf16).reshape(N, LOC, FFP - FFL)
-    s6[:, :, FFP + FFL : 2 * FFP] = jnp.zeros((N, LOC, FFP - FFL), bf16)
+    s6[:, 0, :, FFL:FFP] = tail.astype(bf16).reshape(N, LOC, FFP - FFL)
+    s6[:, 1, :, FFL:FFP] = jnp.zeros((N, LOC, FFP - FFL), bf16)
 
     for r in range(1, N):
         rcopy(s6.at[turn(x, r)], r6.at[r - 1], s6s, r6s, x_to(r), t).start()
     for b in range(N):
         xt5[b] = x5[8 * b : 8 * b + 8].reshape(ROWS, F).astype(f32).T.reshape(2 * Z, 8, ROWS)
     all_here(r6, s6s, r6s)
-    both = s6[x].astype(f32)
+    gate = s6[x, 0].astype(f32)
+    upper = s6[x, 1].astype(f32)
     for i in range(N - 1):
-        both = both + r6[i].astype(f32)
-    total = both[:, FFL : FFL + 1] + both[:, FFL + 1 : FFL + 2]
+        gate = gate + r6[i, 0].astype(f32)
+        upper = upper + r6[i, 1].astype(f32)
+    total = gate[:, FFL : FFL + 1] + gate[:, FFL + 1 : FFL + 2]
     inverse = lax.rsqrt(total / D + EPS)
-    hidden = silu(both[:, 0:FFP] * inverse) * (both[:, FFP : 2 * FFP] * inverse)
+    hidden = silu(gate * inverse) * (upper * inverse)
     spot = lax.broadcasted_iota(jnp.int32, (LOC, FFP), 1)
     h7[x] = jnp.where(spot < FFL, hidden, 0.0).astype(bf16)
 
@@ -285,31 +302,32 @@
     all_here(three(wd), wds, wdr)
     all_here(three(h7), s7s, r7s)
     hall = h7[...].reshape(ROWS, FFP)[:, 0:FFL]
-    for b in range(N):
-        down = jnp.dot(hall, wd[b], preferred_element_type=f32).T
-        for i in range(2 * Z):
-            t8[i % 2, i // 2, b] = down[8 * i : 8 * i + 8, :]
-
-    p8[...] = t8[o].astype(bf16)
-    swap = rcopy(p8, d8, d8s, d8r, k, mate)
-    swap.start()
-    t8[c, z] = t8[c, z] + xt5[:, t]
-    swap.wait_recv()
-    s8[...] = (t8[c] + d8[...].astype(f32)).astype(bf16)
-
-    def piece(r, q):
+    downs = [jnp.dot(hall, wd[b], preferred_element_type=f32).T for b in range(N)]
+    swaps = []
+    for b in range(N):
+        for i in range(Z):
+            even, odd = downs[b][16 * i : 16 * i + 8, :], downs[b][16 * i + 8 : 16 * i + 16, :]
+            t8[i, b] = jnp.where(c == 0, even, odd)
+            p8[b, i] = jnp.where(c == 0, odd, even).astype(bf16)
+        swaps.append(rcopy(p8.at[b], d8.at[b], d8s.at[b], d8r.at[b], k, mate))
+        swaps[b].start()
+
+    def piece(r, there):
         zz = z_to(r)
-        there = turn(y, q)
         rcopy(s8.at[zz, there], r8.at[y * Z + r], s8s, r8s, there * N + x, 2 * zz + c).start()
 
-    def send8(j, _):
-        for q in range(N):
-            piece(z_step(j), q)
-        return 0
-
-    lax.fori_loop(0, Z - 1, send8, 0)
+    t8[z] = t8[z] + xt5[:, t]
+    for b in range(N):
+        swaps[b].wait_recv()
+        s8[:, b] = (t8[:, b] + d8[b].astype(f32)).astype(bf16)
+
+        def send8(j, _):
+            piece(z_step(j), b)
+            return 0
+
+        lax.fori_loop(0, Z - 1, send8, 0)
     for q in range(1, N):
-        piece(0, q)
+        piece(0, turn(y, q))
     r8[y * Z] = s8[z, y]
     pieces = r8.at[pl.ds(0, N * Z - 1)]
     all_here(pieces, s8s, r8s)
@@ -321,12 +339,13 @@
 
     all_sent(three(xa), s0s, r0s)
     all_sent(three(gains), gs, gr)
-    for ref, ss, rs in ((wp, wps, wpr), (wm.at[c], wms, wmr), (wg, wgs, wgr), (wu, wus, wur), (wd, wds, wdr)):
+    for ref, ss, rs in ((wp, wps, wpr), (wo, wos, wor), (wm.at[c], wms, wmr), (wg, wgs, wgr), (wu, wus, wur), (wd, wds, wdr)):
         all_sent(three(ref), ss, rs)
     all_sent(wm.at[c], ms, mr)
     all_sent(x1.at[pl.ds(0, Z - 1)], s1s, r1s.at[0])
     all_sent(x1.at[pl.ds(0, Z)], f1s, f1r)
     all_sent(r2, s2s, r2s)
+    all_sent(r2b, b2s, b2r)
     all_sent(rq2, q2s, q2r)
     all_sent(n3.at[pl.ds(0, 2 * N - 1)], s3s, r3s)
     all_sent(r4, s4s, r4s)
@@ -334,7 +353,8 @@
     all_sent(x5.at[pl.ds(0, Z)], f5s, f5r)
     all_sent(r6, s6s, r6s)
     all_sent(three(h7), s7s, r7s)
-    all_sent(p8, d8s, d8r)
+    for swap in swaps:
+        swap.wait_send()
     all_sent(pieces, s8s, r8s)
 
 
@@ -359,22 +379,23 @@
     hbm = pl.BlockSpec(memory_space=pltpu.HBM)
     V = pltpu.VMEM
     dma = pltpu.SemaphoreType.DMA
-    ring8 = [V((Z, N, 8, ROWS), bf16)] * 3 + [V((N * Z, 8, ROWS), bf16)]
+    ring8 = [V((N, Z, 8, ROWS), bf16)] * 2 + [V((Z, N, 8, ROWS), bf16), V((N * Z, 8, ROWS), bf16)]
     scratch = [
         V((8, 4 * ROWS), bf16), V((1, F), f32), V((1, 128), f32), V((1, 128), f32), V((1, F), f32),
-        V((N, 4, F, 128), bf16), V((2, N, 128, F), bf16), V((N, FFL, F), bf16), V((N, FFL, F), bf16), V((N, FFL, F), bf16),
+        V((N, 3, F, 128), bf16), V((N, F, 128), bf16), V((2, N, 128, F), bf16), V((N, FFL, F), bf16), V((N, FFL, F), bf16), V((N, FFL, F), bf16),
         V((N, 2, F), f32), V((LOC, 128, 128), f32),
         V((N, 8, ROWS), bf16), V((2 * Z, N, 8, ROWS), bf16), V((N, ROWS, F), f32),
-        V((N, LOC, 512), bf16), V((8, ROWS), f32), V((N - 1, LOC, 512), bf16), V((N - 1, 8, ROWS), f32),
+        V((N, LOC, 384), bf16), V((8, ROWS), f32), V((N - 1, LOC, 384), bf16), V((N - 1, 8, ROWS), f32),
+        V((N, LOC, 128), bf16), V((N - 1, LOC, 128), bf16),
         V((128, 128), f32), V((LOC, 128), f32), V((LOC, 128), f32),
         V((2 * N, LOC, 128), bf16),
         V((Z, 16, F), f32), V((Z, 16, F), bf16), V((Z - 1, 16, F), bf16),
         V((16, F), bf16), V((2 * Z, 16, F), bf16), V((N, 2 * Z, 8, ROWS), f32),
-        V((N, LOC, 2 * FFP), bf16), V((N - 1, LOC, 2 * FFP), bf16), V((N, LOC, FFP), bf16),
-        V((2, Z, N, 8, ROWS), f32), *ring8,
-        dma((13,)), dma, *([dma] * 14),
+        V((N, 2, LOC, FFP), bf16), V((N - 1, 2, LOC, FFP), bf16), V((N, LOC, FFP), bf16),
+        V((Z, N, 8, ROWS), f32), *ring8,
+        pltpu.SemaphoreType.REGULAR, dma((13,)), dma, *([dma] * 18),
         dma, dma((Z,)), *([dma] * 12),
-        dma, dma((Z,)), *([dma] * 10),
+        dma, dma((Z,)), *([dma] * 6), dma((N,)), dma((N,)), dma, dma,
     ]
     out, new_state = pl.pallas_call(
         layer_kernel,

time: 82.2 us -> 78.9 us (0.960); the launches traced: 81.1 us -> 78.7 us
  Pallas kernels: 80.5 us -> 78.1 us
    pallas_call x1, Pallas kernels: 79.1 us -> 76.7 us  [body(): pl.pallas_call(layer_kernel, out_shape=(jax.ShapeDtypeStruct((8, 4 * ROWS...]
where the time goes in v4:
time: 78.9 us; the launch traced here: 78.7 us
  Pallas kernels  78.1 us (99%)
    pallas_call x1, Pallas kernels, body(): pl.pallas_call(layer_kernel, out_shape=(jax.ShapeDtypeStruct((8, 4 * ROWS...  76.7 us

profile of v4, /device:TPU:25, one launch (start us, length us, event | category | flops | bytes accessed | tf_op | source)
XLA Modules:
  0.0 78.7 jit_solution(111167508145053553)
XLA Ops:
  0.6 76.7 %shard_map.149 = (bf16[8,512]{1,0:T(8,128)(2,1)S(1)}, f32[32,128,128]{2,1,0:T(8,128)S(1)}) custom-call(bf16[8,512]{1,0:T(8,128)(2,1)} %bitcast.15, f32[1,256]{1,0:T(1,128)} %bitcast.16, f32[1,128]{1,0:T(1,128)} %bitcast.18, f32[1,128]{1,0:T(1,128)} %bitcast.19, f32[1,256]{1,0:T(1,128)} %bitcast.17, bf16[256,128]{1,0:T(8,128)(2,1)} %wq_hbm.1, ...), custom_call_target="tpu_custom_call" | custom-call | tf_op jit(solution)/shard_map/pallas_call | solution.py:400
  77.3 1.4 %shard_map.150 = (bf16[8,512]{1,0:T(8,128)(2,1)}, f32[32,128,128]{2,1,0:T(8,128)}) custom-call(bf16[8,512]{1,0:T(8,128)(2,1)S(1)} %get-tuple-element.6.out_ref, f32[32,128,128]{2,1,0:T(8,128)S(1)} %get-tuple-element.7.ns_ref), custom_call_target="tpu_custom_call" | custom-call | tf_op jit(solution)/shard_map/pallas_call | solution.py:422

commit v5 on v4

--- a/solution.py
+++ b/solution.py
@@ -28,21 +28,15 @@
     return u * sigmoid(u)
 
 
-def z_step(j):
-    sign = 1 - 2 * lax.rem(j, 2)
-    return 8 + sign * ((j + 1) // 2)
-
-
 def layer_kernel(
     x_hbm, mg_hbm, lb_hbm, hg_hbm, fg_hbm,
     wq_hbm, wf_hbm, wi_hbm, wo_hbm, state_hbm, wm_hbm, wg_hbm, wu_hbm, wd_hbm,
     out_ref, ns,
-    x_ref, mg_ref, lb_ref, hg_ref, fg_ref, wp, wo, wm, wg, wu, wd, gains, st,
+    x_ref, mg_ref, lb_ref, hg_ref, fg_ref, wp, wo, wm, wgu, wd, gains, st,
     xa, x1, xf, s2, sq2, r2, rq2, s2b, r2b, qfk, vals, ho, n3, t4, s4, r4, own5, x5, xt5,
     s6, r6, h7, t8, p8, d8, s8, r8,
-    word, wsem, stsem, wps, wpr, wos, wor, wms, wmr, wgs, wgr, wus, wur, wds, wdr, gs, gr, s0s, r0s, b2s, b2r,
-    s1s, r1s, f1s, f1r, s2s, r2s, q2s, q2r, s3s, r3s, ms, mr, s4s, r4s,
-    s5s, r5s, f5s, f5r, s6s, r6s, s7s, r7s, d8s, d8r, s8s, r8s,
+    word, wsem, psem, gsem, stsem, wps, wpr, wos, wor, wms, wmr, wgs, wgr, wds, wdr, gr, r0, ms, mr,
+    out_a, out_b, out_c, ring, fwd, in_a, in_b, in_c, r4s, d8s, d8r, r8s,
 ):
     k = lax.axis_index("kv")
     t = lax.axis_index("tp")
@@ -80,6 +74,9 @@
     def all_here(view, ssem, rsem):
         rcopy(view, view, ssem, rsem, k, mate).wait_recv()
 
+    def unit(n):
+        return r8.at[pl.ds(0, n)]
+
     def three(ref):
         return ref.at[pl.ds(0, N - 1)]
 
@@ -95,64 +92,96 @@
         greet(x_to(r), t)
     greet(k, mate)
 
-    loads = [
-        pltpu.make_async_copy(src, dst, wsem.at[i])
-        for i, (src, dst) in enumerate(
-            (
-                (wq_hbm, wp.at[y, 0]), (wf_hbm, wp.at[y, 1]), (wi_hbm, wp.at[y, 2]), (wo_hbm, wo.at[y]),
-                (wm_hbm, wm.at[c, y]), (wg_hbm, wg.at[y]), (wu_hbm, wu.at[y]), (wd_hbm, wd.at[y]),
-                (x_hbm, x_ref), (mg_hbm, mg_ref), (lb_hbm, lb_ref), (hg_hbm, hg_ref), (fg_hbm, fg_ref),
-            )
-        )
-    ]
-    for load in loads:
+    places = {
+        "x": (x_hbm, x_ref), "mg": (mg_hbm, mg_ref), "fg": (fg_hbm, fg_ref),
+        "o": (wo_hbm, wo.at[y]),
+        "m": (wm_hbm, wm.at[c, y]), "d": (wd_hbm, wd.at[y]),
+        "lb": (lb_hbm, lb_ref), "hg": (hg_hbm, hg_ref),
+    }
+
+    def pass_on(sem, d):
+        for r in (d, Z - d):
+            pl.semaphore_signal(sem, inc=1, device_id=(k, 2 * z_to(r) + c), device_id_type=MESH)
+
+    loads = {
+        name: pltpu.make_async_copy(src, dst, wsem.at[i]) for i, (name, (src, dst)) in enumerate(places.items())
+    }
+    for i, src in enumerate((wq_hbm, wf_hbm, wi_hbm)):
+        pltpu.make_async_copy(src, wp.at[y, i], psem).start()
+    for load in loads.values():
         load.start()
+    for i, src in enumerate((wg_hbm, wu_hbm)):
+        pltpu.make_async_copy(src, wgu.at[y, i], gsem).start()
+    loads["p"] = pltpu.make_async_copy(wp.at[y], wp.at[y], psem)
+    loads["g"] = pltpu.make_async_copy(wgu.at[y], wgu.at[y], gsem)
+    loads["x"].wait()
+    pl.semaphore_wait(pltpu.get_barrier_semaphore(), 8 + 2 * (N - 1) + 1)
+    for r in range(1, N):
+        there = turn(y, r)
+        lanes = pl.ds(pl.multiple_of(there * ROWS, ROWS), ROWS)
+        rcopy(x_ref.at[:, lanes], xa.at[y], out_a, r0, y_to(r), t).start()
+    pass_on(word, 4)
+    loads["mg"].wait()
+    loads["fg"].wait()
+    gains[y, 0:1, :] = mg_ref[...]
+    gains[y, 1:2, :] = fg_ref[...]
+    for r in range(1, N):
+        rcopy(gains.at[y], gains.at[y], out_a, gr, y_to(r), t).start()
+    weights = (
+        ("p", wp, wps, wpr), ("o", wo, wos, wor), ("m", wm.at[c], wms, wmr), ("g", wgu, wgs, wgr), ("d", wd, wds, wdr),
+    )
+
+    def send_weights(name, ref, ss, rs):
+        third = FFL // 3
+        if name == "p":
+            parts = [ref.at[y, i] for i in range(3)]
+        elif name == "g":
+            parts = [ref.at[y, i, pl.ds(third * j, third)] for i in range(2) for j in range(3)]
+        elif name == "d":
+            parts = [ref.at[y, pl.ds(third * j, third)] for j in range(3)]
+        else:
+            parts = [ref.at[y]]
+        for part in parts:
+            for r in range(1, N):
+                rcopy(part, part, ss, rs, y_to(r), t).start()
+
+    for name, ref, ss, rs in weights:
+        loads[name].wait()
+        send_weights(name, ref, ss, rs)
     state_in = pltpu.make_async_copy(state_hbm, st, stsem)
     state_in.start()
-    for load in loads:
-        load.wait()
-    gains[y, 0:1, :] = mg_ref[...]
-    gains[y, 1:2, :] = fg_ref[...]
-    pl.semaphore_wait(pltpu.get_barrier_semaphore(), 8 + 2 * (N - 1) + 1)
-
-    pl.semaphore_signal(word, inc=1, device_id=(k, 2 * z_to(4) + c), device_id_type=MESH)
-    pl.semaphore_signal(word, inc=1, device_id=(k, 2 * z_to(Z - 4) + c), device_id_type=MESH)
-
-    for r in range(1, N):
-        there = turn(y, r)
-        lanes = pl.ds(pl.multiple_of(there * ROWS, ROWS), ROWS)
-        rcopy(x_ref.at[:, lanes], xa.at[y], s0s, r0s, y_to(r), t).start()
-        rcopy(gains.at[y], gains.at[y], gs, gr, y_to(r), t).start()
-    for ref, ss, rs in ((wp, wps, wpr), (wo, wos, wor), (wm.at[c], wms, wmr), (wg, wgs, wgr), (wu, wus, wur), (wd, wds, wdr)):
-        for r in range(1, N):
-            rcopy(ref.at[y], ref.at[y], ss, rs, y_to(r), t).start()
+    loads["lb"].wait()
+    loads["hg"].wait()
     mine = pl.ds(pl.multiple_of(y * ROWS, ROWS), ROWS)
     xa[y] = x_ref[:, mine]
-    all_here(three(xa), s0s, r0s)
+    all_here(three(xa), out_a, r0)
+
+    def ways(d):
+        return (d, Z - d) if d < 8 else (8,)
+
+    def to_far(own, slots, slot, out):
+        for d in range(8, 0, -1):
+            for r in ways(d):
+                rcopy(own, slots.at[slot(z, c)], out, ring.at[d - 1], k, 2 * z_to(r) + c).start()
+
+    def pass_to_mate(own, slots, slot, out):
+        rcopy(own, slots.at[slot(z, c)], out, fwd, k, mate).start()
+        for d in range(1, 9):
+            all_here(slots.at[pl.ds(0, len(ways(d)))], out, ring.at[d - 1])
+            for r in ways(d):
+                src = slots.at[slot(z_from(r), c)]
+                rcopy(src, src, out, fwd, k, mate).start()
+        all_here(slots.at[pl.ds(0, Z)], out, fwd)
+
+    x1[t] = xa[...]
+
+    def by_tp(zz, cc):
+        return 2 * zz + cc
+
     pl.semaphore_wait(word, 2)
-
-    def gather_tp(own, slots, slot, ss, rs, fs, fr):
-        def send(j, _):
-            r = z_step(j)
-            rcopy(own, slots.at[slot(z, c)], ss, rs.at[r], k, 2 * z_to(r) + c).start()
-            return 0
-
-        lax.fori_loop(0, Z - 1, send, 0)
-        rcopy(own, slots.at[slot(z, c)], fs, fr, k, mate).start()
-
-        def forward(i, _):
-            r = z_step(Z - 2 - i)
-            src = slot(z_from(r), c)
-            rcopy(own, slots.at[src], ss, rs.at[r], k, mate).wait_recv()
-            rcopy(slots.at[src], slots.at[src], fs, fr, k, mate).start()
-            return 0
-
-        lax.fori_loop(0, Z - 1, forward, 0)
-        all_here(slots.at[pl.ds(0, Z)], fs, fr)
-
-    x1[t] = xa[...]
-    gather_tp(xa, x1, lambda zz, cc: 2 * zz + cc, s1s, r1s, f1s, f1r)
-    all_here(three(gains), gs, gr)
+    to_far(xa, x1, by_tp, out_b)
+    pass_to_mate(xa, x1, by_tp, out_b)
+    all_here(three(gains), out_a, gr)
     all_here(three(wp), wps, wpr)
 
     row = jnp.zeros((1, ROWS), f32)
@@ -175,17 +204,14 @@
         s2[:, :, 128 * i : 128 * i + 128] = projection(lambda b, i=i: wp[b, i])
 
     for r in range(1, N):
-        rcopy(s2.at[turn(x, r)], r2.at[r - 1], s2s, r2s, x_to(r), t).start()
-        rcopy(sq2, rq2.at[r - 1], q2s, q2r, x_to(r), t).start()
+        rcopy(s2.at[turn(x, r)], r2.at[r - 1], out_c, in_a, x_to(r), t).start()
+        rcopy(sq2, rq2.at[r - 1], out_c, in_a, x_to(r), t).start()
     all_here(three(wo), wos, wor)
     s2b[...] = projection(lambda b: wo[b])
     for r in range(1, N):
-        rcopy(s2b.at[turn(x, r)], r2b.at[r - 1], b2s, b2r, x_to(r), t).start()
-    all_here(three(wm.at[c]), wms, wmr)
-    rcopy(wm.at[c], wm.at[c], ms, mr, k, mate).start()
+        rcopy(s2b.at[turn(x, r)], r2b.at[r - 1], out_c, in_b, x_to(r), t).start()
     state_in.wait()
-    all_here(rq2, q2s, q2r)
-    all_here(r2, s2s, r2s)
+    all_here(unit(42), out_c, in_a)
 
     sq = sq2[...]
     raw = s2[x].astype(f32)
@@ -210,7 +236,7 @@
     for s in range(LOC):
         ho[s : s + 1, :] = jnp.sum(qfk[:, s : s + 1] * st[s], axis=0, keepdims=True)
 
-    all_here(r2b, b2s, b2r)
+    all_here(r2b, out_c, in_b)
     raw = s2b[x].astype(f32)
     for i in range(N - 1):
         raw = raw + r2b[i].astype(f32)
@@ -220,17 +246,20 @@
     n3[2 * x + c] = (head * inv * hg_ref[...] * out_gate).astype(bf16)
 
     mine3 = n3.at[2 * x + c]
-    for r in range(1, N):
-        rcopy(mine3, mine3, s3s, r3s, x_to(r), t).start()
-        rcopy(mine3, mine3, s3s, r3s, x_to(r), mate).start()
-    rcopy(mine3, mine3, s3s, r3s, k, mate).start()
+    all_sent(unit(6), out_a, in_c)
+    for r in range(1, N):
+        rcopy(mine3, mine3, out_a, in_c, x_to(r), t).start()
+        rcopy(mine3, mine3, out_a, in_c, x_to(r), mate).start()
+    rcopy(mine3, mine3, out_a, in_c, k, mate).start()
+    all_here(three(wm.at[c]), wms, wmr)
+    rcopy(wm.at[c], wm.at[c], ms, mr, k, mate).start()
     for s in range(LOC):
         ns[s] = (
             qfk[:, LOC + s : LOC + s + 1] * st[s]
             + qfk[:, 2 * LOC + s : 2 * LOC + s + 1] * vals[s : s + 1, :]
         )
     all_here(wm.at[o], ms, mr)
-    all_here(n3.at[pl.ds(0, 2 * N - 1)], s3s, r3s)
+    all_here(n3.at[pl.ds(0, 2 * N - 1)], out_a, in_c)
 
     heads = [jnp.concatenate([n3[4 * c + i], n3[4 * c + 2 + i]], axis=0) for i in range(2)]
     for b in range(N):
@@ -243,22 +272,20 @@
     def block_of(zz, cc):
         return (zz // 4) * 8 + cc * 4 + lax.rem(zz, 4)
 
-    def send4(j, _):
-        r = z_step(j)
-        zz = z_to(r)
-        rcopy(s4.at[zz], r4.at[r - 1], s4s, r4s, k, 2 * zz + c).start()
-        return 0
-
-    lax.fori_loop(0, Z - 1, send4, 0)
+    all_sent(x1.at[pl.ds(0, 2 * Z - 1)], out_b, in_c)
+    for d in range(8, 0, -1):
+        for r in ways(d):
+            rcopy(s4.at[z_to(r)], r4.at[r - 1], out_b, r4s, k, 2 * z_to(r) + c).start()
     block = xf[z // 4, pl.ds(pl.multiple_of(c * 64 + lax.rem(z, 4) * 16, 16), 16), :] + t4[z]
-    all_here(r4, s4s, r4s)
+    all_here(r4, out_b, r4s)
     for i in range(Z - 1):
         block = block + r4[i].astype(f32)
     own5[...] = block.astype(bf16)
     x5[block_of(z, c)] = own5[...]
-    gather_tp(own5, x5, block_of, s5s, r5s, f5s, f5r)
-    all_here(three(wg), wgs, wgr)
-    all_here(three(wu), wus, wur)
+    all_sent(unit(54), out_c, r4s)
+    to_far(own5, x5, block_of, out_c)
+    pass_to_mate(own5, x5, block_of, out_c)
+    all_here(three(wgu), wgs, wgr)
 
     squares = jnp.zeros((ROWS, 1), f32)
     scaled = []
@@ -267,25 +294,26 @@
         squares = squares + jnp.sum(after * after, axis=1, keepdims=True)
         scaled.append((after * gains[b, 1:2, :]).astype(bf16))
 
-    def projected(w):
-        acc = lax.dot_general(scaled[0], w[0], NT, preferred_element_type=f32)
+    def projected(i):
+        acc = lax.dot_general(scaled[0], wgu[0, i], NT, preferred_element_type=f32)
         for b in range(1, N):
-            acc = acc + lax.dot_general(scaled[b], w[b], NT, preferred_element_type=f32)
+            acc = acc + lax.dot_general(scaled[b], wgu[b, i], NT, preferred_element_type=f32)
         return acc.astype(bf16).reshape(N, LOC, FFL)
 
-    s6[:, 0, :, 0:FFL] = projected(wg)
-    s6[:, 1, :, 0:FFL] = projected(wu)
+    s6[:, 0, :, 0:FFL] = projected(0)
+    s6[:, 1, :, 0:FFL] = projected(1)
     high = squares.astype(bf16).astype(f32)
     spot = lax.broadcasted_iota(jnp.int32, (ROWS, FFP - FFL), 1)
     tail = jnp.where(spot == 0, high, jnp.where(spot == 1, squares - high, 0.0))
     s6[:, 0, :, FFL:FFP] = tail.astype(bf16).reshape(N, LOC, FFP - FFL)
     s6[:, 1, :, FFL:FFP] = jnp.zeros((N, LOC, FFP - FFL), bf16)
 
-    for r in range(1, N):
-        rcopy(s6.at[turn(x, r)], r6.at[r - 1], s6s, r6s, x_to(r), t).start()
+    all_sent(unit(28), out_a, in_a)
+    for r in range(1, N):
+        rcopy(s6.at[turn(x, r)], r6.at[r - 1], out_a, in_a, x_to(r), t).start()
     for b in range(N):
         xt5[b] = x5[8 * b : 8 * b + 8].reshape(ROWS, F).astype(f32).T.reshape(2 * Z, 8, ROWS)
-    all_here(r6, s6s, r6s)
+    all_here(r6, out_a, in_a)
     gate = s6[x, 0].astype(f32)
     upper = s6[x, 1].astype(f32)
     for i in range(N - 1):
@@ -297,10 +325,11 @@
     spot = lax.broadcasted_iota(jnp.int32, (LOC, FFP), 1)
     h7[x] = jnp.where(spot < FFL, hidden, 0.0).astype(bf16)
 
-    for r in range(1, N):
-        rcopy(h7.at[x], h7.at[x], s7s, r7s, x_to(r), t).start()
+    all_sent(unit(60), out_b, in_b)
+    for r in range(1, N):
+        rcopy(h7.at[x], h7.at[x], out_b, in_b, x_to(r), t).start()
     all_here(three(wd), wds, wdr)
-    all_here(three(h7), s7s, r7s)
+    all_here(three(h7), out_b, in_b)
     hall = h7[...].reshape(ROWS, FFP)[:, 0:FFL]
     downs = [jnp.dot(hall, wd[b], preferred_element_type=f32).T for b in range(N)]
     swaps = []
@@ -309,53 +338,39 @@
             even, odd = downs[b][16 * i : 16 * i + 8, :], downs[b][16 * i + 8 : 16 * i + 16, :]
             t8[i, b] = jnp.where(c == 0, even, odd)
             p8[b, i] = jnp.where(c == 0, odd, even).astype(bf16)
-        swaps.append(rcopy(p8.at[b], d8.at[b], d8s.at[b], d8r.at[b], k, mate))
+        swaps.append(rcopy(p8.at[b], d8.at[b], d8s, d8r.at[b], k, mate))
         swaps[b].start()
+
+    all_sent(x5.at[pl.ds(0, 2 * Z - 1)], out_c, in_b)
 
     def piece(r, there):
         zz = z_to(r)
-        rcopy(s8.at[zz, there], r8.at[y * Z + r], s8s, r8s, there * N + x, 2 * zz + c).start()
+        rcopy(s8.at[zz, there], r8.at[y * Z + r], out_c, r8s, there * N + x, 2 * zz + c).start()
 
     t8[z] = t8[z] + xt5[:, t]
     for b in range(N):
         swaps[b].wait_recv()
         s8[:, b] = (t8[:, b] + d8[b].astype(f32)).astype(bf16)
-
-        def send8(j, _):
-            piece(z_step(j), b)
-            return 0
-
-        lax.fori_loop(0, Z - 1, send8, 0)
+        for d in range(8, 0, -1):
+            for r in ways(d):
+                piece(r, b)
     for q in range(1, N):
         piece(0, turn(y, q))
     r8[y * Z] = s8[z, y]
-    pieces = r8.at[pl.ds(0, N * Z - 1)]
-    all_here(pieces, s8s, r8s)
+    all_here(unit(N * Z - 1), out_c, r8s)
     for b in range(N):
         acc = r8[b * Z].astype(f32)
         for i in range(1, Z):
             acc = acc + r8[b * Z + i].astype(f32)
         out_ref[:, ROWS * b : ROWS * b + ROWS] = acc.astype(bf16)
 
-    all_sent(three(xa), s0s, r0s)
-    all_sent(three(gains), gs, gr)
-    for ref, ss, rs in ((wp, wps, wpr), (wo, wos, wor), (wm.at[c], wms, wmr), (wg, wgs, wgr), (wu, wus, wur), (wd, wds, wdr)):
+    for _, ref, ss, rs in weights:
         all_sent(three(ref), ss, rs)
     all_sent(wm.at[c], ms, mr)
-    all_sent(x1.at[pl.ds(0, Z - 1)], s1s, r1s.at[0])
-    all_sent(x1.at[pl.ds(0, Z)], f1s, f1r)
-    all_sent(r2, s2s, r2s)
-    all_sent(r2b, b2s, b2r)
-    all_sent(rq2, q2s, q2r)
-    all_sent(n3.at[pl.ds(0, 2 * N - 1)], s3s, r3s)
-    all_sent(r4, s4s, r4s)
-    all_sent(x5.at[pl.ds(0, Z - 1)], s5s, r5s.at[0])
-    all_sent(x5.at[pl.ds(0, Z)], f5s, f5r)
-    all_sent(r6, s6s, r6s)
-    all_sent(three(h7), s7s, r7s)
-    for swap in swaps:
-        swap.wait_send()
-    all_sent(pieces, s8s, r8s)
+    all_sent(unit(N * Z), d8s, r8s)
+    all_sent(r6, out_a, in_a)
+    all_sent(three(h7), out_b, in_b)
+    all_sent(unit(N * Z - 1), out_c, r8s)
 
 
 def write_out(out_ref, ns_ref, out_hbm, ns_hbm, sems):
@@ -382,7 +397,7 @@
     ring8 = [V((N, Z, 8, ROWS), bf16)] * 2 + [V((Z, N, 8, ROWS), bf16), V((N * Z, 8, ROWS), bf16)]
     scratch = [
         V((8, 4 * ROWS), bf16), V((1, F), f32), V((1, 128), f32), V((1, 128), f32), V((1, F), f32),
-        V((N, 3, F, 128), bf16), V((N, F, 128), bf16), V((2, N, 128, F), bf16), V((N, FFL, F), bf16), V((N, FFL, F), bf16), V((N, FFL, F), bf16),
+        V((N, 3, F, 128), bf16), V((N, F, 128), bf16), V((2, N, 128, F), bf16), V((N, 2, FFL, F), bf16), V((N, FFL, F), bf16),
         V((N, 2, F), f32), V((LOC, 128, 128), f32),
         V((N, 8, ROWS), bf16), V((2 * Z, N, 8, ROWS), bf16), V((N, ROWS, F), f32),
         V((N, LOC, 384), bf16), V((8, ROWS), f32), V((N - 1, LOC, 384), bf16), V((N - 1, 8, ROWS), f32),
@@ -393,9 +408,8 @@
         V((16, F), bf16), V((2 * Z, 16, F), bf16), V((N, 2 * Z, 8, ROWS), f32),
         V((N, 2, LOC, FFP), bf16), V((N - 1, 2, LOC, FFP), bf16), V((N, LOC, FFP), bf16),
         V((Z, N, 8, ROWS), f32), *ring8,
-        pltpu.SemaphoreType.REGULAR, dma((13,)), dma, *([dma] * 18),
-        dma, dma((Z,)), *([dma] * 12),
-        dma, dma((Z,)), *([dma] * 6), dma((N,)), dma((N,)), dma, dma,
+        pltpu.SemaphoreType.REGULAR, dma((8,)), *([dma] * 17),
+        dma, dma, dma, dma((8,)), *([dma] * 6), dma((N,)), dma,
     ]
     out, new_state = pl.pallas_call(
         layer_kernel,

time: 78.9 us -> 76.1 us (0.965)
  Pallas kernels: 78.1 us -> 75.3 us
    pallas_call x1, Pallas kernels: 76.7 us -> 73.9 us  [body(): pl.pallas_call(layer_kernel, out_shape=(jax.ShapeDtypeStruct((8, 4 * ROWS...]
where the time goes in v5:
time: 76.1 us; the launch traced here: 75.9 us
  Pallas kernels  75.3 us (99%)
    pallas_call x1, Pallas kernels, body(): pl.pallas_call(layer_kernel, out_shape=(jax.ShapeDtypeStruct((8, 4 * ROWS...  73.9 us

profile of v5, /device:TPU:25, one launch (start us, length us, event | category | flops | bytes accessed | tf_op | source)
XLA Modules:
  0.0 75.9 jit_solution(8738149214656535453)
XLA Ops:
  0.6 73.9 %shard_map.149 = (bf16[8,512]{1,0:T(8,128)(2,1)S(1)}, f32[32,128,128]{2,1,0:T(8,128)S(1)}) custom-call(bf16[8,512]{1,0:T(8,128)(2,1)} %bitcast.15, f32[1,256]{1,0:T(1,128)} %bitcast.16, f32[1,128]{1,0:T(1,128)} %bitcast.18, f32[1,128]{1,0:T(1,128)} %bitcast.19, f32[1,256]{1,0:T(1,128)} %bitcast.17, bf16[256,128]{1,0:T(8,128)(2,1)} %wq_hbm.1, ...), custom_call_target="tpu_custom_call" | custom-call | tf_op jit(solution)/shard_map/pallas_call | solution.py:414
  74.6 1.4 %shard_map.150 = (bf16[8,512]{1,0:T(8,128)(2,1)}, f32[32,128,128]{2,1,0:T(8,128)}) custom-call(bf16[8,512]{1,0:T(8,128)(2,1)S(1)} %get-tuple-element.6.out_ref, f32[32,128,128]{2,1,0:T(8,128)S(1)} %get-tuple-element.7.ns_ref), custom_call_target="tpu_custom_call" | custom-call | tf_op jit(solution)/shard_map/pallas_call | solution.py:436

commit v6 on v5

--- a/solution.py
+++ b/solution.py
@@ -87,7 +87,7 @@
     for d in range(4, 0, -1):
         greet(k, 2 * z_to(d) + c)
         greet(k, 2 * z_to(Z - d) + c)
-    for r in range(1, N):
+    for r in (2, 1, 3):
         greet(y_to(r), t)
         greet(x_to(r), t)
     greet(k, mate)
@@ -116,7 +116,7 @@
     loads["g"] = pltpu.make_async_copy(wgu.at[y], wgu.at[y], gsem)
     loads["x"].wait()
     pl.semaphore_wait(pltpu.get_barrier_semaphore(), 8 + 2 * (N - 1) + 1)
-    for r in range(1, N):
+    for r in (2, 1, 3):
         there = turn(y, r)
         lanes = pl.ds(pl.multiple_of(there * ROWS, ROWS), ROWS)
         rcopy(x_ref.at[:, lanes], xa.at[y], out_a, r0, y_to(r), t).start()
@@ -125,7 +125,7 @@
     loads["fg"].wait()
     gains[y, 0:1, :] = mg_ref[...]
     gains[y, 1:2, :] = fg_ref[...]
-    for r in range(1, N):
+    for r in (2, 1, 3):
         rcopy(gains.at[y], gains.at[y], out_a, gr, y_to(r), t).start()
     weights = (
         ("p", wp, wps, wpr), ("o", wo, wos, wor), ("m", wm.at[c], wms, wmr), ("g", wgu, wgs, wgr), ("d", wd, wds, wdr),
@@ -142,7 +142,7 @@
         else:
             parts = [ref.at[y]]
         for part in parts:
-            for r in range(1, N):
+            for r in (2, 1, 3):
                 rcopy(part, part, ss, rs, y_to(r), t).start()
 
     for name, ref, ss, rs in weights:
@@ -203,12 +203,12 @@
     for i in range(3):
         s2[:, :, 128 * i : 128 * i + 128] = projection(lambda b, i=i: wp[b, i])
 
-    for r in range(1, N):
+    for r in (2, 1, 3):
         rcopy(s2.at[turn(x, r)], r2.at[r - 1], out_c, in_a, x_to(r), t).start()
         rcopy(sq2, rq2.at[r - 1], out_c, in_a, x_to(r), t).start()
     all_here(three(wo), wos, wor)
     s2b[...] = projection(lambda b: wo[b])
-    for r in range(1, N):
+    for r in (2, 1, 3):
         rcopy(s2b.at[turn(x, r)], r2b.at[r - 1], out_c, in_b, x_to(r), t).start()
     state_in.wait()
     all_here(unit(42), out_c, in_a)
@@ -247,12 +247,13 @@
 
     mine3 = n3.at[2 * x + c]
     all_sent(unit(6), out_a, in_c)
-    for r in range(1, N):
+    for r in (2, 1, 3):
+        rcopy(mine3, mine3, out_a, in_c, x_to(r), mate).start()
         rcopy(mine3, mine3, out_a, in_c, x_to(r), t).start()
-        rcopy(mine3, mine3, out_a, in_c, x_to(r), mate).start()
     rcopy(mine3, mine3, out_a, in_c, k, mate).start()
     all_here(three(wm.at[c]), wms, wmr)
-    rcopy(wm.at[c], wm.at[c], ms, mr, k, mate).start()
+    for b in range(N):
+        rcopy(wm.at[c, b], wm.at[c, b], ms, mr, k, mate).start()
     for s in range(LOC):
         ns[s] = (
             qfk[:, LOC + s : LOC + s + 1] * st[s]
@@ -309,7 +310,7 @@
     s6[:, 1, :, FFL:FFP] = jnp.zeros((N, LOC, FFP - FFL), bf16)
 
     all_sent(unit(28), out_a, in_a)
-    for r in range(1, N):
+    for r in (2, 1, 3):
         rcopy(s6.at[turn(x, r)], r6.at[r - 1], out_a, in_a, x_to(r), t).start()
     for b in range(N):
         xt5[b] = x5[8 * b : 8 * b + 8].reshape(ROWS, F).astype(f32).T.reshape(2 * Z, 8, ROWS)
@@ -326,7 +327,7 @@
     h7[x] = jnp.where(spot < FFL, hidden, 0.0).astype(bf16)
 
     all_sent(unit(60), out_b, in_b)
-    for r in range(1, N):
+    for r in (2, 1, 3):
         rcopy(h7.at[x], h7.at[x], out_b, in_b, x_to(r), t).start()
     all_here(three(wd), wds, wdr)
     all_here(three(h7), out_b, in_b)

time: 76.1 us -> 76.1 us (level)
  no operation moved by 1% of the time
where the time goes in v6:
time: 76.1 us; the launch traced here: 75.9 us
  Pallas kernels  75.3 us (99%)
    pallas_call x1, Pallas kernels, body(): pl.pallas_call(layer_kernel, out_shape=(jax.ShapeDtypeStruct((8, 4 * ROWS...  73.9 us

profile of v6, /device:TPU:25, one launch (start us, length us, event | category | flops | bytes accessed | tf_op | source)
XLA Modules:
  0.0 75.9 jit_solution(4902429052703679741)
XLA Ops:
  0.6 73.9 %shard_map.149 = (bf16[8,512]{1,0:T(8,128)(2,1)S(1)}, f32[32,128,128]{2,1,0:T(8,128)S(1)}) custom-call(bf16[8,512]{1,0:T(8,128)(2,1)} %bitcast.15, f32[1,256]{1,0:T(1,128)} %bitcast.16, f32[1,128]{1,0:T(1,128)} %bitcast.18, f32[1,128]{1,0:T(1,128)} %bitcast.19, f32[1,256]{1,0:T(1,128)} %bitcast.17, bf16[256,128]{1,0:T(8,128)(2,1)} %wq_hbm.1, ...), custom_call_target="tpu_custom_call" | custom-call | tf_op jit(solution)/shard_map/pallas_call | solution.py:415
  74.6 1.4 %shard_map.150 = (bf16[8,512]{1,0:T(8,128)(2,1)}, f32[32,128,128]{2,1,0:T(8,128)}) custom-call(bf16[8,512]{1,0:T(8,128)(2,1)S(1)} %get-tuple-element.6.out_ref, f32[32,128,128]{2,1,0:T(8,128)S(1)} %get-tuple-element.7.ns_ref), custom_call_target="tpu_custom_call" | custom-call | tf_op jit(solution)/shard_map/pallas_call | solution.py:437

commit v7 on v6

--- a/solution.py
+++ b/solution.py
@@ -248,12 +248,11 @@
     mine3 = n3.at[2 * x + c]
     all_sent(unit(6), out_a, in_c)
     for r in (2, 1, 3):
+        rcopy(mine3, mine3, out_a, in_c, x_to(r), t).start()
         rcopy(mine3, mine3, out_a, in_c, x_to(r), mate).start()
-        rcopy(mine3, mine3, out_a, in_c, x_to(r), t).start()
     rcopy(mine3, mine3, out_a, in_c, k, mate).start()
     all_here(three(wm.at[c]), wms, wmr)
-    for b in range(N):
-        rcopy(wm.at[c, b], wm.at[c, b], ms, mr, k, mate).start()
+    rcopy(wm.at[c], wm.at[c], ms, mr, k, mate).start()
     for s in range(LOC):
         ns[s] = (
             qfk[:, LOC + s : LOC + s + 1] * st[s]

time: 76.1 us -> 75.5 us (level)
  no operation moved by 1% of the time
where the time goes in v7:
time: 75.5 us; the launch traced here: 75.4 us
  Pallas kernels  74.8 us (99%)
    pallas_call x1, Pallas kernels, body(): pl.pallas_call(layer_kernel, out_shape=(jax.ShapeDtypeStruct((8, 4 * ROWS...  73.4 us

profile of v7, /device:TPU:25, one launch (start us, length us, event | category | flops | bytes accessed | tf_op | source)
XLA Modules:
  0.0 75.4 jit_solution(16310735651870389880)
XLA Ops:
  0.6 73.4 %shard_map.149 = (bf16[8,512]{1,0:T(8,128)(2,1)S(1)}, f32[32,128,128]{2,1,0:T(8,128)S(1)}) custom-call(bf16[8,512]{1,0:T(8,128)(2,1)} %bitcast.15, f32[1,256]{1,0:T(1,128)} %bitcast.16, f32[1,128]{1,0:T(1,128)} %bitcast.18, f32[1,128]{1,0:T(1,128)} %bitcast.19, f32[1,256]{1,0:T(1,128)} %bitcast.17, bf16[256,128]{1,0:T(8,128)(2,1)} %wq_hbm.1, ...), custom_call_target="tpu_custom_call" | custom-call | tf_op jit(solution)/shard_map/pallas_call | solution.py:414
  74.0 1.4 %shard_map.150 = (bf16[8,512]{1,0:T(8,128)(2,1)}, f32[32,128,128]{2,1,0:T(8,128)}) custom-call(bf16[8,512]{1,0:T(8,128)(2,1)S(1)} %get-tuple-element.6.out_ref, f32[32,128,128]{2,1,0:T(8,128)S(1)} %get-tuple-element.7.ns_ref), custom_call_target="tpu_custom_call" | custom-call | tf_op jit(solution)/shard_map/pallas_call | solution.py:436
